TPU v7x, 32 devices: a whole 2x2x4 slice. The times are simulated.
32 devices in a mesh: sp: 4 (over z), fs: 4 (over y, core), tp: 2 (over x).
Axes of the slice: x: 2, y: 2, z: 4, core: 2. Of those that a mesh axis runs over, the one named last changes fastest.
Arguments:
- tokens: bfloat16 [4096, 2048], P(('fs', 'sp', 'tp')), parts along dimension 0, may hold values from -6 to 6
- norm_gain: bfloat16 [2048], replicated, may hold values from 0.099609375 to 1.8984375
- w_pool_in: bfloat16 [2048, 1024], P('sp', 'tp'), may hold values from -0.125 to 0.125
- w_query: bfloat16 [2048, 1024], P('sp', 'tp'), may hold values from -0.125 to 0.125
- w_key: bfloat16 [2048, 1024], P('sp', 'tp'), may hold values from -0.125 to 0.125
- w_value: bfloat16 [2048, 1024], P('sp', 'tp'), may hold values from -0.125 to 0.125
- w_gate: bfloat16 [2048, 1024], P('sp', 'tp'), may hold values from -0.125 to 0.125
- w_beta: bfloat16 [2048, 8], replicated, may hold values from -0.125 to 0.125
- w_decay: bfloat16 [2048, 8], replicated, may hold values from -0.5 to 0.5
- conv_weight: float32 [3, 4, 1024], P(None, None, 'tp'), may hold values from -3 to 3
- a_log: float32 [8], P('tp'), may hold values from -20 to -1.7, as said below
- decay_extra: float32 [4096, 8], P(('fs', 'sp'), 'tp'), parts along dimension 0, may hold values from -1.4 to 0
- w_mix: bfloat16 [8, 128, 128], P('tp'), may hold values from -0.5 to 0.5
- pool_scale: float32 [1024], P('tp'), may hold values from 0.1 to 1.9
- delta_gain: float32 [128], replicated, may hold values from 0.1 to 1.9
- w_out_pool: bfloat16 [1024, 2048], P('tp', 'sp'), may hold values from -0.125 to 0.125
- w_out_delta: bfloat16 [1024, 2048], P('tp', 'sp'), may hold values from -0.125 to 0.125
Outputs:
- mixed: bfloat16 [4096, 2048], P(('fs', 'sp', 'tp')), parts along dimension 0
There are 4 independent parts, one for each index of `fs`. A program takes and returns all parts, laid end to end along the dimension named above; an argument that names none is the same for every part. Nothing has to cross between parts.
Inputs may be any that keep to these rules, and one draw needn't show every extreme that they name: `a_log`: logarithm of each head's base decay rate.
All inputs are finite; a program needn't handle non-finite values.
Results may differ from a plain program's by a relative error of at most 0.018.
Values may be sent and summed in bfloat16 or wider, within the bound.
A program may use at most 64 MiB of HBM per device.

v0:
```python
import jax
import jax.numpy as jnp
from jax import lax
from jax.sharding import PartitionSpec as P

BLOCK = 64


eps = 1e-06
windows = (2, 4, 8, 16)
tail_rows = 15
highest = lax.Precision.HIGHEST


def from_behind(block, axis, distance):
    devices = range(lax.axis_size(axis))
    route = [(i - distance, i) for i in devices if i - distance in devices]
    return lax.ppermute(block, axis, route)


def rms_rows(values, gain):
    floats = values.astype(jnp.float32)
    scale = lax.rsqrt(jnp.mean(floats * floats, axis=-1, keepdims=True) + eps)
    return (floats * scale * gain.astype(jnp.float32)).astype(jnp.bfloat16)


def unit_rows(values):
    return values * lax.rsqrt(jnp.sum(values * values, axis=-1, keepdims=True) + eps)


def block_terms(query, keys, values, log_gate, strength, block):
    heads, length, width = keys.shape
    count = length // block

    def split(tensor):
        return tensor.reshape(heads, count, block, tensor.shape[-1])

    query_part, key_part, value_part = (split(query), split(keys), split(values))
    gate_cum = jnp.cumsum(log_gate.reshape(heads, count, block), axis=-1)
    beta_part = strength.reshape(heads, count, block)[..., None]
    lower_mask = jnp.tril(jnp.ones((block, block), dtype=bool))
    strict_mask = jnp.tril(jnp.ones((block, block), dtype=bool), k=-1)
    gaps = gate_cum[..., :, None] - gate_cum[..., None, :]
    decay_tab = jnp.where(lower_mask, jnp.exp(jnp.where(lower_mask, gaps, 0.0)), 0.0)
    key_scaled_beta = key_part * beta_part
    value_beta = value_part * beta_part
    corr_lower = jnp.where(
        strict_mask,
        jnp.einsum("hnid,hnjd->hnij", key_scaled_beta, key_part, precision=highest) * decay_tab,
        0.0,
    )
    identity = jnp.eye(block, dtype=jnp.float32)
    inverse = lax.linalg.triangular_solve(
        identity + corr_lower,
        jnp.broadcast_to(identity, corr_lower.shape),
        left_side=True,
        lower=True,
    )
    fixed_values = jnp.einsum("hnij,hnjd->hnid", inverse, value_beta, precision=highest)
    key_weights = jnp.einsum(
        "hnij,hnjd->hnid",
        inverse,
        key_scaled_beta * jnp.exp(gate_cum)[..., None],
        precision=highest,
    )
    scores = jnp.where(
        lower_mask,
        jnp.einsum("hnid,hnjd->hnij", query_part, key_part, precision=highest) * decay_tab,
        0.0,
    )
    key_decayed = key_part * jnp.exp(gate_cum[..., -1:] - gate_cum)[..., None]
    query_gated = query_part * jnp.exp(gate_cum)[..., None]
    terms = (query_gated, key_decayed, fixed_values, key_weights, scores, gate_cum[..., -1])
    return tuple((jnp.moveaxis(tensor, 1, 0) for tensor in terms))


def carry_step(state, inputs):
    query_gated, key_decayed, fixed_values, key_weights, scores, last_gate = inputs
    fresh = fixed_values - jnp.einsum("hcd,hde->hce", key_weights, state, precision=highest)
    output = jnp.einsum("hcd,hde->hce", query_gated, state, precision=highest) + jnp.einsum(
        "hij,hje->hie", scores, fresh, precision=highest
    )
    state = state * jnp.exp(last_gate)[:, None, None] + jnp.einsum(
        "hcd,hce->hde", key_decayed, fresh, precision=highest
    )
    return (state, output)


def compose_step(carry, inputs):
    linear, offset = carry
    query_gated, key_decayed, fixed_values, key_weights, scores, last_gate = inputs
    fade = jnp.exp(last_gate)[:, None, None]
    moved = jnp.einsum("hcd,hde->hce", key_weights, linear, precision=highest)
    linear = fade * linear - jnp.einsum("hcd,hce->hde", key_decayed, moved, precision=highest)
    fresh = fixed_values - jnp.einsum("hcd,hde->hce", key_weights, offset, precision=highest)
    offset = fade * offset + jnp.einsum("hcd,hce->hde", key_decayed, fresh, precision=highest)
    return ((linear, offset), None)


def apply_map(linear, state):
    return jnp.einsum("hij,hjk->hik", linear, state, precision=highest)


def per_device(
    tokens,
    norm_gain,
    w_pool_in,
    w_query,
    w_key,
    w_value,
    w_gate,
    w_beta,
    w_decay,
    conv_weight,
    a_log,
    decay_extra,
    w_mix,
    pool_scale,
    delta_gain,
    w_out_pool,
    w_out_delta,
):
    pool_w, query_w, key_w, value_w, gate_w, outp_w, outd_w = (
        lax.all_gather(w_pool_in, "sp", axis=0, tiled=True),
        lax.all_gather(w_query, "sp", axis=0, tiled=True),
        lax.all_gather(w_key, "sp", axis=0, tiled=True),
        lax.all_gather(w_value, "sp", axis=0, tiled=True),
        lax.all_gather(w_gate, "sp", axis=0, tiled=True),
        lax.all_gather(w_out_pool, "sp", axis=1, tiled=True),
        lax.all_gather(w_out_delta, "sp", axis=1, tiled=True),
    )
    rows_all = lax.all_gather(tokens, "tp", axis=0, tiled=True)
    norm_result = rms_rows(rows_all, norm_gain)
    length = norm_result.shape[0]

    def project(weight):
        return jnp.dot(norm_result, weight, preferred_element_type=jnp.float32).astype(jnp.bfloat16)

    pool_in = project(pool_w)
    query_raw = project(query_w)
    key_raw = project(key_w)
    value_raw = project(value_w)
    gate_raw = project(gate_w)
    heads_dev = a_log.shape[0]
    head_dim = query_raw.shape[1] // heads_dev
    width_dev = heads_dev * head_dim
    all_heads = w_beta.shape[1]
    lane = lax.axis_index("tp")
    both_pre = jnp.dot(
        norm_result, jnp.concatenate([w_beta, w_decay], axis=1), preferred_element_type=jnp.float32
    )
    beta_pre = lax.dynamic_slice_in_dim(both_pre[:, :all_heads], lane * heads_dev, heads_dev, 1)
    forget_logits = lax.dynamic_slice_in_dim(
        both_pre[:, all_heads:], lane * heads_dev, heads_dev, 1
    )
    raw_three = jnp.concatenate([query_raw, key_raw, value_raw], axis=1)
    tails = jnp.concatenate(
        [pool_in[length - tail_rows :], raw_three[length - tail_rows :]], axis=1
    )
    prior_state = from_behind(tails, "sp", 1)
    pool_width_dev = pool_in.shape[1]
    source_rows = pool_in.astype(jnp.float32)
    extended = jnp.concatenate(
        [prior_state[:, :pool_width_dev].astype(jnp.float32), source_rows], axis=0
    )
    running = jnp.concatenate(
        [jnp.zeros((1, pool_width_dev), jnp.float32), jnp.cumsum(extended, axis=0)], axis=0
    )
    groups_dev = w_mix.shape[0]
    group_dim = w_mix.shape[1]
    group = lane * groups_dev + jnp.arange(pool_width_dev) // group_dim
    span = (2 ** (1 + group % 4)).astype(jnp.int32)
    ending = running[tail_rows + 1 : tail_rows + 1 + length]
    window_sum = jnp.zeros((length, pool_width_dev), jnp.float32)
    for width in windows:
        lagged = running[tail_rows + 1 - width : tail_rows + 1 - width + length]
        window_sum = window_sum + jnp.where(span[None, :] == width, ending - lagged, 0.0)
    positions = lax.axis_index("sp") * length + jnp.arange(length)
    counts = jnp.minimum(positions[:, None] + 1, span[None, :]).astype(jnp.float32)
    pooled = (window_sum / counts - source_rows).astype(jnp.bfloat16)
    mixed_pool = jnp.einsum(
        "sgc,gcd->sgd",
        pooled.reshape(length, groups_dev, group_dim),
        w_mix,
        preferred_element_type=jnp.float32,
    )
    pool_out = (mixed_pool.reshape(length, pool_width_dev) * pool_scale).astype(jnp.bfloat16)
    taps = conv_weight.shape[1]
    kernel = jnp.transpose(conv_weight, (1, 0, 2)).reshape(taps, 3 * width_dev)
    stacked = jnp.concatenate(
        [prior_state[tail_rows - (taps - 1) :, pool_width_dev:], raw_three], axis=0
    ).astype(jnp.float32)
    conv = jnp.zeros((length, 3 * width_dev), jnp.float32)
    for tap in range(taps):
        conv = conv + stacked[tap : tap + length] * kernel[tap]
    after_silu = jax.nn.silu(conv)

    def heads_first(tensor):
        return jnp.transpose(tensor.reshape(length, heads_dev, head_dim), (1, 0, 2))

    query = unit_rows(heads_first(after_silu[:, :width_dev])) * head_dim ** (-0.5)
    keys = unit_rows(heads_first(after_silu[:, width_dev : 2 * width_dev]))
    values = heads_first(after_silu[:, 2 * width_dev :])
    strength = jax.nn.sigmoid(beta_pre).T
    log_gate = (-jnp.exp(a_log)[None, :] * jax.nn.softplus(forget_logits) + decay_extra).T
    terms = block_terms(query, keys, values, log_gate, strength, BLOCK)
    identity = jnp.broadcast_to(
        jnp.eye(head_dim, dtype=jnp.float32), (heads_dev, head_dim, head_dim)
    )
    empty = jnp.zeros((heads_dev, head_dim, head_dim), jnp.float32)
    (linear, offset), _ = lax.scan(compose_step, (identity, empty), terms)

    def advance(turn, arriving):
        return from_behind(
            (apply_map(linear, arriving) + offset).astype(jnp.bfloat16), "sp", 1
        ).astype(jnp.float32)

    incoming = lax.fori_loop(0, lax.axis_size("sp") - 1, advance, empty)
    _, outputs = lax.scan(carry_step, incoming, terms)
    attended = jnp.transpose(outputs, (1, 0, 2, 3)).reshape(heads_dev, length, head_dim)
    normal_out = (
        attended
        * lax.rsqrt(jnp.mean(attended * attended, axis=-1, keepdims=True) + eps)
        * delta_gain
    )
    gated = normal_out * jax.nn.silu(heads_first(gate_raw.astype(jnp.float32)))
    delta_out = jnp.transpose(gated, (1, 0, 2)).reshape(length, width_dev).astype(jnp.bfloat16)
    value_partial_rows = jnp.dot(pool_out, outp_w, preferred_element_type=jnp.float32) + jnp.dot(
        delta_out, outd_w, preferred_element_type=jnp.float32
    )
    return lax.psum_scatter(
        lax.optimization_barrier(value_partial_rows.astype(jnp.bfloat16))
        .astype(jnp.float32)
        .astype(jnp.bfloat16),
        "tp",
        scatter_dimension=0,
        tiled=True,
    )


def solution(mesh):
    placed = (
        P(("fs", "sp", "tp"), None),
        P(),
        P("sp", "tp"),
        P("sp", "tp"),
        P("sp", "tp"),
        P("sp", "tp"),
        P("sp", "tp"),
        P(),
        P(),
        P(None, None, "tp"),
        P("tp"),
        P(("fs", "sp"), "tp"),
        P("tp", None, None),
        P("tp"),
        P(),
        P("tp", "sp"),
        P("tp", "sp"),
    )
    return jax.shard_map(
        per_device,
        mesh=mesh,
        in_specs=placed,
        out_specs=P(("fs", "sp", "tp"), None),
        check_vma=False,
    )
```

profile of v0, /device:TPU:31, one launch (start us, length us, event | category | flops | bytes accessed | tf_op | source)
XLA Modules:
  0.0 431.4 jit_solution(9990838366187681166)
XLA Ops:
  6.5 0.7 all-gather.9.cloned.1.call-update
  7.3 0.7 all-gather.11.cloned.1.call-update
  8.1 0.7 all-gather.17.cloned.1.call-update
  9.4 0.5 all-gather.13.cloned.1.call-update
  10.6 0.7 all-gather.19.cloned.1.call-update
  11.3 0.7 all-gather.23.cloned.1.call-update
  12.5 17.5 %all-gather.9.cloned.1.call-done = bf16[256,2048]{1,0:T(8,128)(2,1)} async-done(((bf16[128,2048]{1,0:T(8,128)(2,1)}), bf16[256,2048]{1,0:T(8,128)(2,1)}) %all-gather.9.cloned.1.call-update) | async-done | bytes 1048592 | tf_op jit(solution)/shard_map/all_gather | solution.py:132
  30.0 1.6 fusion.42
  31.7 1.7 fusion.102
  33.5 0.9 reduce_window_sum.28
  34.9 41.4 %all-gather.11.cloned.1.call-done = bf16[2048,512]{1,0:T(8,128)(2,1)} async-done(((bf16[512,512]{1,0:T(8,128)(2,1)}), bf16[2048,512]{1,0:T(8,128)(2,1)}) %all-gather.11.cloned.1.call-update) | async-done | bytes 2097168 | tf_op jit(solution)/shard_map/all_gather | solution.py:124
  76.3 3.1 fusion.127
  79.5 42.9 %all-gather.17.cloned.1.call-done = bf16[2048,512]{1,0:T(8,128)(2,1)} async-done(((bf16[512,512]{1,0:T(8,128)(2,1)}), bf16[2048,512]{1,0:T(8,128)(2,1)}) %all-gather.17.cloned.1.call-update) | async-done | bytes 2097168 | tf_op jit(solution)/shard_map/all_gather | solution.py:127
  122.4 2.3 convolution_convert_fusion.1
  124.7 43.6 %all-gather.15.cloned.1.call-done = bf16[2048,512]{1,0:T(8,128)(2,1)} async-done(((bf16[512,512]{1,0:T(8,128)(2,1)}), bf16[2048,512]{1,0:T(8,128)(2,1)}) %all-gather.15.cloned.1.call-update) | async-done | bytes 2097168 | tf_op jit(solution)/shard_map/all_gather | solution.py:126
  168.3 2.3 convolution_convert_fusion.2
  170.6 43.6 %all-gather.13.cloned.1.call-done = bf16[2048,512]{1,0:T(8,128)(2,1)} async-done(((bf16[512,512]{1,0:T(8,128)(2,1)}), bf16[2048,512]{1,0:T(8,128)(2,1)}) %all-gather.13.cloned.1.call-update) | async-done | bytes 2097168 | tf_op jit(solution)/shard_map/all_gather | solution.py:125
  214.2 2.3 convolution_convert_fusion.3
  216.6 1.3 collective-permute-start.1
  217.9 42.3 %all-gather.21.cloned.1.call-done = bf16[2048,512]{1,0:T(8,128)(2,1)} async-done(((bf16[512,512]{1,0:T(8,128)(2,1)}), bf16[2048,512]{1,0:T(8,128)(2,1)}) %all-gather.21.cloned.1.call-update) | async-done | bytes 2097168 | tf_op jit(solution)/shard_map/all_gather | solution.py:128
  260.1 3.1 fusion.55
  263.5 0.9 divide_multiply_fusion
  265.6 1.8 fusion.53
  267.4 1.0 fusion.51
  268.4 78.8 %custom-call.3 = f32[4,4,1,64,64]{3,4,2,1,0:T(8,128)S(1)} custom-call(f32[4,4,1,64,64]{4,3,2,1,0:T(8,128)S(1)} %fusion.51), custom_call_target="InvertDiagBlocksLowerTriangular" | custom-call | tf_op jit(solution)/shard_map/triangular_solve | solution.py:53
  347.2 1.0 fusion.85
  348.3 0.9 convolution_bitcast_fusion.2
  349.2 0.7 convolution_bitcast_fusion.1
  350.3 8.1 %while.37 = (s32[]{:T(128)}, f32[4,128,128]{2,1,0:T(8,128)S(1)}, f32[4,128,128]{2,1,0:T(8,128)S(1)}, f32[4,4]{1,0:T(4,128)S(1)}, f32[4,4,64,128]{3,2,1,0:T(8,128...) while((s32[]{:T(128)}, f32[4,128,128]{2,1,0:T(8,128)S(1)}, ...), condition=%wide.region_6.7_spmd.clone, body=%wide.region_5.6_spmd.clone.sunk | while | flops 201752576 | bytes 2754712 | solution.py:211
  350.7 0.6 convolution_add_fusion.8
  351.6 0.6 convolution_subtract_fusion.7
  352.7 0.6 convolution_add_fusion.8
  353.7 0.6 convolution_subtract_fusion.7
  354.7 0.6 convolution_add_fusion.8
  355.7 0.6 convolution_subtract_fusion.7
  356.7 0.6 convolution_add_fusion.8
  357.7 0.6 convolution_subtract_fusion.7
  358.4 19.1 %while.38 = (s32[]{:T(128)}, f32[4,128,128]{2,1,0:T(8,128)S(1)}, f32[4,128,128]{2,1,0:T(8,128)S(1)}, f32[4,128,128]{2,1,0:T(8,128)S(1)}, s32[]{:T(128)}, /*index=5*/s32[]{:T(128)}) while((s32[]{:T(128)}, f32[4,128,128]{2,1,0:T(8,128)S(1)}, f32[4,128,128]{2,1,0:T(8,128)S(1)}, f32[4,128,128]{2,1,0:T(8,128)S(1)}, s32[]{:T(128)}, ...), condition=%wide.region_8.9_spmd.clone, body=%wide.region_7.8_spmd.clone.sunk | while | flops 100925440 | bytes 1835127 | solution.py:218
  358.8 1.3 collective-permute-start
  360.1 5.1 %collective-permute-done = bf16[4,128,128]{2,1,0:T(8,128)(2,1)S(1)} collective-permute-done((bf16[4,128,128]{2,1,0:T(8,128)(2,1)S(1)}, bf16[4,128,128]{2,1,0:T(8,128)(2,1)S(1)}, u32[]{:S(2)}, u32[]{:S(2)}) %collective-permute-start) | collective-permute-done | bytes 131104 | tf_op jit(solution)/shard_map/while/body/eval_jaxpr/ppermute | solution.py:18
  365.6 1.3 collective-permute-start
  366.9 4.4 %collective-permute-done = bf16[4,128,128]{2,1,0:T(8,128)(2,1)S(1)} collective-permute-done((bf16[4,128,128]{2,1,0:T(8,128)(2,1)S(1)}, bf16[4,128,128]{2,1,0:T(8,128)(2,1)S(1)}, u32[]{:S(2)}, u32[]{:S(2)}) %collective-permute-start) | collective-permute-done | bytes 131104 | tf_op jit(solution)/shard_map/while/body/eval_jaxpr/ppermute | solution.py:18
  371.8 1.3 collective-permute-start
  373.1 4.4 %collective-permute-done = bf16[4,128,128]{2,1,0:T(8,128)(2,1)S(1)} collective-permute-done((bf16[4,128,128]{2,1,0:T(8,128)(2,1)S(1)}, bf16[4,128,128]{2,1,0:T(8,128)(2,1)S(1)}, u32[]{:S(2)}, u32[]{:S(2)}) %collective-permute-start) | collective-permute-done | bytes 131104 | tf_op jit(solution)/shard_map/while/body/eval_jaxpr/ppermute | solution.py:18
  377.5 12.8 %while.36 = (s32[]{:T(128)}, f32[4,128,128]{2,1,0:T(8,128)S(1)}, f32[4,4,64,128]{3,2,0,1:T(8,128)}, f32[4,4]{1,0:T(4,128)S(1)}, f32[4,4,64,128]{3,2,1,0:T(8,128)...) while((s32[]{:T(128)}, f32[4,128,128]{2,1,0:T(8,128)S(1)}, ...), condition=%wide.region_11.12_spmd, body=%wide.region_10.11_spmd.sunk | while | flops 176357376 | bytes 2493581 | solution.py:219
  377.9 1.2 fusion.185
  379.1 1.0 fusion.186
  380.1 0.6 convolution_add_fusion.7
  381.1 1.2 fusion.185
  382.3 1.0 fusion.186
  383.3 0.6 convolution_add_fusion.7
  384.3 1.2 fusion.185
  385.5 1.0 fusion.186
  386.5 0.6 convolution_add_fusion.7
  387.5 1.2 fusion.185
  388.7 1.0 fusion.186
  389.7 0.6 convolution_add_fusion.7
  390.4 1.3 fusion.84
  391.8 1.3 fusion.90
  393.4 0.5 fusion.56
  395.0 0.6 fusion.92
  395.8 2.3 fusion.128
  398.2 3.3 fusion.41
  401.5 23.4 %reduce-scatter.2.cloned.1.call-done = bf16[128,2048]{1,0:T(8,128)(2,1)} async-done(((bf16[256,2048]{1,0:T(8,128)(2,1)}), bf16[128,2048]{1,0:T(8,128)(2,1)}) %reduce-scatter.2.cloned.1.call-update) | async-done | bytes 524304 | tf_op jit(solution)/shard_map/reduce_scatter | solution.py:231
  (125 shorter events, 11.2 us)
Async XLA Ops:
  6.5 388.0 %copy-start = (bf16[4,128,128]{2,1,0:T(8,128)(2,1)S(1)}, bf16[4,128,128]{2,1,0:T(8,128)(2,1)}, u32[]{:S(2)}) copy-start(bf16[4,128,128]{2,1,0:T(8,128)(2,1)} %param.35) | copy-start | bytes 393220
  6.5 5.7 %copy-start.5 = (bf16[2048]{0:T(1024)(128)(2,1)S(1)}, bf16[2048]{0:T(1024)(128)(2,1)}, u32[]{:S(2)}) copy-start(bf16[2048]{0:T(1024)(128)(2,1)} %param.24) | copy-start | bytes 12292
  6.5 5.7 %copy-start.4 = (f32[3,4,512]{2,1,0:T(4,128)S(1)}, f32[3,4,512]{2,1,0:T(4,128)}, u32[]{:S(2)}) copy-start(f32[3,4,512]{2,1,0:T(4,128)} %param.32) | copy-start | bytes 73732
  6.5 23.5 %all-gather.9.cloned.1.call-start = ((), (), s32[]{:S(2)}) async-start(), calls=%async_computation.1 | async-start | bytes 1572864 | tf_op jit(solution)/shard_map/all_gather | solution.py:132
  7.3 5.1 %copy-start.13 = (f32[4]{0:T(128)S(1)}, f32[4]{0:T(128)}, u32[]{:S(2)}) copy-start(f32[4]{0:T(128)} %param.33) | copy-start | bytes 52
  7.3 69.0 %all-gather.11.cloned.1.call-start = ((), (), s32[]{:S(2)}) async-start(), calls=%async_computation.2 | async-start | bytes 2621440 | tf_op jit(solution)/shard_map/all_gather | solution.py:124
  8.0 114.4 %all-gather.17.cloned.1.call-start = ((), (), s32[]{:S(2)}) async-start(), calls=%async_computation.5 | async-start | bytes 2621440 | tf_op jit(solution)/shard_map/all_gather | solution.py:127
  8.8 22.9 %copy-start.11 = (bf16[2048,8]{0,1:T(8,128)(2,1)S(1)}, bf16[2048,8]{0,1:T(8,128)(2,1)}, u32[]{:S(2)}) copy-start(bf16[2048,8]{0,1:T(8,128)(2,1)} %param.31) | copy-start | bytes 98308
  8.8 22.9 %copy-start.12 = (bf16[2048,8]{0,1:T(8,128)(2,1)S(1)}, bf16[2048,8]{0,1:T(8,128)(2,1)}, u32[]{:S(2)}) copy-start(bf16[2048,8]{0,1:T(8,128)(2,1)} %param.30) | copy-start | bytes 98308
  8.8 159.5 %all-gather.15.cloned.1.call-start = ((), (), s32[]{:S(2)}) async-start(), calls=%async_computation.4 | async-start | bytes 2621440 | tf_op jit(solution)/shard_map/all_gather | solution.py:126
  9.4 204.9 %all-gather.13.cloned.1.call-start = ((), (), s32[]{:S(2)}) async-start(), calls=%async_computation.3 | async-start | bytes 2621440 | tf_op jit(solution)/shard_map/all_gather | solution.py:125
  9.9 250.2 %all-gather.21.cloned.1.call-start = ((), (), s32[]{:S(2)}) async-start(), calls=%async_computation.7 | async-start | bytes 2621440 | tf_op jit(solution)/shard_map/all_gather | solution.py:128
  10.5 22.8 %copy-start.6 = (f32[256,4]{0,1:T(4,128)S(1)}, f32[256,4]{0,1:T(4,128)}, u32[]{:S(2)}) copy-start(f32[256,4]{0,1:T(4,128)} %param.34) | copy-start | bytes 12292
  10.5 385.3 %all-gather.19.cloned.1.call-start = ((), (), s32[]{:S(2)}) async-start(), calls=%async_computation.6 | async-start | bytes 2621440 | tf_op jit(solution)/shard_map/all_gather | solution.py:129
  11.3 386.9 %all-gather.23.cloned.1.call-start = ((), (), s32[]{:S(2)}) async-start(), calls=%async_computation.8 | async-start | bytes 2621440 | tf_op jit(solution)/shard_map/all_gather | solution.py:130
  12.0 412.9 %reduce-scatter.2.cloned.1.call-start = ((), (), s32[]{:S(2)}) async-start(), calls=%async_computation.9 | async-start | bytes 1572864 | tf_op jit(solution)/shard_map/reduce_scatter | solution.py:231
  30.0 46.3 %copy-start.1 = (bf16[256,2048]{1,0:T(8,128)(2,1)S(1)}, bf16[256,2048]{1,0:T(8,128)(2,1)}, u32[]{:S(2)}) copy-start(bf16[256,2048]{1,0:T(8,128)(2,1)} %all-gather.9.cloned.1.call-done) | copy-start | bytes 3145732
  79.4 45.3 %copy-start.8 = (bf16[256,512]{1,0:T(8,128)(2,1)}, bf16[256,512]{1,0:T(8,128)(2,1)S(1)}, u32[]{:S(2)}) copy-start(bf16[256,512]{1,0:T(8,128)(2,1)S(1)} %get-tuple-element.255) | copy-start | bytes 786436
  216.6 46.7 %collective-permute-start.1 = (bf16[15,2048]{1,0:T(8,128)(2,1)S(1)}, bf16[15,2048]{1,0:T(8,128)(2,1)S(1)}, u32[]{:S(2)}, u32[]{:S(2)}) collective-permute-start(bf16[15,2048]{1,0:T(8,128)(2,1)S(1)} %fusion.101), channel_id=1, source_target_pairs={{0,8},{8,16},{16,24},{1,9},{9,17},{17,25},{2,10},{10,18},{18,26},{... | collective-permute-start | bytes 184328 | tf_op jit(solution)/shard_map/ppermute | solution.py:18
  358.8 6.4 %collective-permute-start = (bf16[4,128,128]{2,1,0:T(8,128)(2,1)S(1)}, bf16[4,128,128]{2,1,0:T(8,128)(2,1)S(1)}, u32[]{:S(2)}, u32[]{:S(2)}) collective-permute-start(bf16[4,128,128]{2,1,0:T(8,128)(2,1)S(1)} %fusion.199), channel_id=1, source_target_pairs={{0,8},{8,16},{16,24},{1,9},{9,17},{17,25},{2,10},{10,18},{18,26},{... | collective-permute-start | bytes 393224 | tf_op jit(solution)/shard_map/while/body/eval_jaxpr/ppermute | solution.py:18
  365.6 5.7 %collective-permute-start = (bf16[4,128,128]{2,1,0:T(8,128)(2,1)S(1)}, bf16[4,128,128]{2,1,0:T(8,128)(2,1)S(1)}, u32[]{:S(2)}, u32[]{:S(2)}) collective-permute-start(bf16[4,128,128]{2,1,0:T(8,128)(2,1)S(1)} %fusion.199), channel_id=1, source_target_pairs={{0,8},{8,16},{16,24},{1,9},{9,17},{17,25},{2,10},{10,18},{18,26},{... | collective-permute-start | bytes 393224 | tf_op jit(solution)/shard_map/while/body/eval_jaxpr/ppermute | solution.py:18
  371.8 5.7 %collective-permute-start = (bf16[4,128,128]{2,1,0:T(8,128)(2,1)S(1)}, bf16[4,128,128]{2,1,0:T(8,128)(2,1)S(1)}, u32[]{:S(2)}, u32[]{:S(2)}) collective-permute-start(bf16[4,128,128]{2,1,0:T(8,128)(2,1)S(1)} %fusion.199), channel_id=1, source_target_pairs={{0,8},{8,16},{16,24},{1,9},{9,17},{17,25},{2,10},{10,18},{18,26},{... | collective-permute-start | bytes 393224 | tf_op jit(solution)/shard_map/while/body/eval_jaxpr/ppermute | solution.py:18
  377.5 14.3 %copy-start.2 = (f32[32,4,8,128]{3,2,1,0:T(8,128)S(1)}, f32[32,4,8,128]{3,2,1,0:T(8,128)}, u32[]{:S(2)}) copy-start(f32[32,4,8,128]{3,2,1,0:T(8,128)} %fusion.55) | copy-start | bytes 1572868
  377.5 14.3 %copy-start.10 = (f32[128]{0:T(128)S(1)}, f32[128]{0:T(128)}, u32[]{:S(2)}) copy-start(f32[128]{0:T(128)} %param.37) | copy-start | bytes 1540
  390.4 2.9 copy-start.3
  394.0 1.0 copy-start.9
  395.0 0.7 copy-start.7
Sparse Core Ops, SparseCore 0:
  8.9 21.0 all-gather.8
  31.6 44.6 all-gather.10
  77.9 44.4 all-gather.16
  123.8 44.4 all-gather.14
  169.7 44.4 all-gather.12
  215.6 44.4 all-gather.20
  261.7 44.5 all-gather.18
  307.8 44.9 all-gather.22
  401.6 23.2 reduce-scatter.1
where the time goes:
time: 435 us; the launch traced here: 431 us
  waiting for transfers between devices  274 us (63%)
  other arithmetic  87.7 us (20%)
  matrix products  48.3 us (11%)
  between operations  13.7 us (3%)
  starting transfers between devices  5.47 us (1%)
    another operation x1, other arithmetic, block_terms(): lax.linalg.triangular_solve(identity + corr_lower, jnp.broadcast_to(ident...  78.8 us
    all_gather x1, waiting for transfers between devices, per_device(): lax.all_gather(w_query, 'sp', axis=0, tiled=True)  43.6 us
    all_gather x1, waiting for transfers between devices, per_device(): lax.all_gather(w_key, 'sp', axis=0, tiled=True)  43.6 us
    all_gather x1, waiting for transfers between devices, per_device(): lax.all_gather(w_value, 'sp', axis=0, tiled=True)  42.9 us
    all_gather x1, waiting for transfers between devices, per_device(): lax.all_gather(w_gate, 'sp', axis=0, tiled=True)  42.3 us
    all_gather x1, waiting for transfers between devices, per_device(): lax.all_gather(w_pool_in, 'sp', axis=0, tiled=True)  41.4 us
    reduce_scatter x1, waiting for transfers between devices, per_device(): lax.psum_scatter(lax.optimization_barrier(value_partial_rows.astype(jnp.b...  23.4 us
    all_gather x1, waiting for transfers between devices, per_device(): rows_all = lax.all_gather(tokens, 'tp', axis=0, tiled=True)  17.5 us
  transfers between devices with their start and end apart: 13, of which 10 were waited for; matrix products, arithmetic and copies ran while one was open for 31% of the time, Pallas kernels for 0%

commit v1 on v0

--- a/solution.py
+++ b/solution.py
@@ -1,6 +1,10 @@
+import functools
+
 import jax
 import jax.numpy as jnp
 from jax import lax
+from jax.experimental import pallas as pl
+from jax.experimental.pallas import tpu as pltpu
 from jax.sharding import PartitionSpec as P
 
 BLOCK = 64
@@ -10,6 +14,295 @@
 windows = (2, 4, 8, 16)
 tail_rows = 15
 highest = lax.Precision.HIGHEST
+
+
+MESH = pl.DeviceIdType.MESH
+halo = 16
+
+
+def share_bits(n_fs):
+    if n_fs & (n_fs - 1):
+        return []
+    return [n_fs >> (k + 1) for k in range(n_fs.bit_length() - 1)]
+
+
+class Gather:
+    def __init__(self, n_sp, n_fs, wbuf, z_s, z_r, f_s, f_r):
+        self.n_sp, self.bits = n_sp, share_bits(n_fs)
+        self.wbuf, self.z_s, self.z_r, self.f_s, self.f_r = wbuf, z_s, z_r, f_s, f_r
+        self.sp, self.fs = lax.axis_index("sp"), lax.axis_index("fs")
+        self.pieces = 2 ** len(self.bits)
+        self.mine = self.fs if self.bits else 0 * self.fs
+        self.depth = wbuf.shape[2] // self.pieces
+
+    def partner(self, bit):
+        return self.fs + bit * (1 - 2 * (self.fs // bit % 2))
+
+    def mask_of(self, m, index):
+        for i, bit in enumerate(self.bits):
+            if m >> i & 1:
+                index = index + bit * (1 - 2 * (index // bit % 2))
+        return index
+
+    def piece(self, w, src, index):
+        return self.wbuf.at[w, src, pl.ds(pl.multiple_of(index * self.depth, self.depth), self.depth)]
+
+    def z_copy(self, w, d, src):
+        ref = self.piece(w, src, self.mine)
+        return pltpu.make_async_remote_copy(
+            src_ref=ref, dst_ref=ref, send_sem=self.z_s.at[w, d - 1], recv_sem=self.z_r.at[w, d - 1],
+            device_id={"sp": lax.rem(self.sp + d, self.n_sp)}, device_id_type=MESH)
+
+    def source(self, d):
+        return lax.rem(self.sp - d + self.n_sp, self.n_sp)
+
+    def f_copy(self, w, d, k, m):
+        slot = 2 ** k - 1 + m
+        ref = self.piece(w, self.source(d), self.mask_of(m, self.mine))
+        return pltpu.make_async_remote_copy(
+            src_ref=ref, dst_ref=ref, send_sem=self.f_s.at[w, d - 1, slot], recv_sem=self.f_r.at[w, d - 1, slot],
+            device_id={"fs": self.partner(self.bits[k])}, device_id_type=MESH)
+
+    def send(self, w):
+        def body(d, c):
+            self.z_copy(w, d, self.sp).start()
+            return c
+        lax.fori_loop(1, self.n_sp, body, 0)
+
+    def arrive_z(self, w, d):
+        self.z_copy(w, d, self.source(d)).wait_recv()
+        for k in range(len(self.bits)):
+            self.f_copy(w, d, k, 0).start()
+
+    def arrive_f(self, w, d, k):
+        for m in range(2 ** k):
+            self.f_copy(w, d, k, m).wait_recv()
+            for later in range(k + 1, len(self.bits)):
+                self.f_copy(w, d, later, m | 1 << k).start()
+
+    def forward(self, w):
+        last = self.n_sp - 1
+        inner = len(self.bits) - 1
+
+        def body(d, c):
+            self.arrive_z(w, d)
+            for k in range(inner):
+                if w == 0:
+                    @pl.when(d > 1)
+                    def _():
+                        self.arrive_f(w, d - 1, k)
+                else:
+                    @pl.when(d > 1)
+                    def _():
+                        self.arrive_f(w, d - 1, k)
+
+                    @pl.when(d == 1)
+                    def _():
+                        self.arrive_f(w - 1, last, k)
+            return c
+        lax.fori_loop(1, self.n_sp, body, 0)
+
+    def flush(self, w):
+        for k in range(len(self.bits) - 1):
+            self.arrive_f(w, self.n_sp - 1, k)
+
+    def finish(self, w):
+        if self.bits:
+            def body(d, c):
+                self.arrive_f(w, d, len(self.bits) - 1)
+                return c
+            lax.fori_loop(1, self.n_sp, body, 0)
+
+    def drain(self, w):
+        def body(d, c):
+            self.z_copy(w, d, self.sp).wait_send()
+            for k in range(len(self.bits)):
+                for m in range(2 ** k):
+                    self.f_copy(w, d, k, m).wait_send()
+            return c
+        lax.fori_loop(1, self.n_sp, body, 0)
+
+
+def enter(n_sp, n_fs, n_tp):
+    sp, fs, tp = (lax.axis_index(a) for a in ("sp", "fs", "tp"))
+    barrier = pltpu.get_barrier_semaphore()
+    bits = share_bits(n_fs)
+    for d in range(1, n_sp):
+        pl.semaphore_signal(barrier, inc=1, device_id={"sp": lax.rem(sp + d, n_sp)}, device_id_type=MESH)
+    for bit in bits:
+        pl.semaphore_signal(barrier, inc=1, device_id={"fs": fs + bit * (1 - 2 * (fs // bit % 2))}, device_id_type=MESH)
+    for d in range(1, n_tp):
+        pl.semaphore_signal(barrier, inc=1, device_id={"tp": lax.rem(tp + d, n_tp)}, device_id_type=MESH)
+    pl.semaphore_wait(barrier, n_sp - 1 + len(bits) + n_tp - 1)
+
+
+def gather_tokens(n_sp, n_tp, tokbuf, rows, tok_s, tok_r, halo_s, halo_r):
+    sp, tp = lax.axis_index("sp"), lax.axis_index("tp")
+
+    def tok_copy(d, owner):
+        ref = tokbuf.at[pl.ds(pl.multiple_of(halo + owner * rows, 16), rows)]
+        return pltpu.make_async_remote_copy(
+            src_ref=ref, dst_ref=ref, send_sem=tok_s.at[d - 1], recv_sem=tok_r.at[d - 1],
+            device_id={"tp": lax.rem(tp + d, n_tp)}, device_id_type=MESH)
+
+    def halo_next():
+        return pltpu.make_async_remote_copy(
+            src_ref=tokbuf.at[pl.ds(n_tp * rows, halo)], dst_ref=tokbuf.at[pl.ds(0, halo)],
+            send_sem=halo_s.at[0], recv_sem=halo_r.at[0],
+            device_id={"sp": lax.rem(sp + 1, n_sp)}, device_id_type=MESH)
+
+    def halo_side(d):
+        ref = tokbuf.at[pl.ds(0, halo)]
+        return pltpu.make_async_remote_copy(
+            src_ref=ref, dst_ref=ref, send_sem=halo_s.at[d], recv_sem=halo_r.at[d],
+            device_id={"tp": lax.rem(tp + d, n_tp)}, device_id_type=MESH)
+
+    end = n_tp - 1
+
+    def start():
+        for d in range(1, n_tp):
+            tok_copy(d, tp).start()
+
+        @pl.when(jnp.logical_and(tp == end, sp < n_sp - 1))
+        def _():
+            halo_next().start()
+
+        @pl.when(sp == 0)
+        def _():
+            tokbuf[0:halo, :] = jnp.zeros((halo, tokbuf.shape[1]), tokbuf.dtype)
+
+    def finish():
+        @pl.when(jnp.logical_and(tp == end, sp > 0))
+        def _():
+            halo_next().wait_recv()
+            for d in range(1, n_tp):
+                halo_side(d).start()
+        for d in range(1, n_tp):
+            tok_copy(d, lax.rem(tp - d + n_tp, n_tp)).wait_recv()
+
+        @pl.when(jnp.logical_and(tp < end, sp > 0))
+        def _():
+            for d in range(1, n_tp):
+                @pl.when(tp == d - 1)
+                def _():
+                    halo_side(d).wait_recv()
+
+    def drain():
+        for d in range(1, n_tp):
+            tok_copy(d, tp).wait_send()
+
+        @pl.when(jnp.logical_and(tp == end, sp < n_sp - 1))
+        def _():
+            halo_next().wait_send()
+
+        @pl.when(jnp.logical_and(tp == end, sp > 0))
+        def _():
+            for d in range(1, n_tp):
+                halo_side(d).wait_send()
+
+    return start, finish, drain
+
+
+def project_kernel(n_sp, n_fs, n_tp, *refs):
+    tok_ref, gain_ref, wbd_ref = refs[:3]
+    w_refs = refs[3:10]
+    proj_ref, pre_ref, wo_ref = refs[10:13]
+    tokbuf, normbuf, wbuf, loc, tok_s, tok_r, halo_s, halo_r, z_s, z_r, f_s, f_r = refs[13:]
+    rows, width = tok_ref.shape
+    sp, tp = lax.axis_index("sp"), lax.axis_index("tp")
+    count = len(w_refs)
+    local = [pltpu.make_async_copy(w_refs[i], wbuf.at[i, sp], loc.at[i]) for i in range(count)]
+    here = pltpu.make_async_copy(
+        tok_ref, tokbuf.at[pl.ds(pl.multiple_of(halo + tp * rows, 16), rows)], loc.at[count])
+    here.start()
+    for copy in local:
+        copy.start()
+    enter(n_sp, n_fs, n_tp)
+    start, finish, drain = gather_tokens(n_sp, n_tp, tokbuf, rows, tok_s, tok_r, halo_s, halo_r)
+    gather = Gather(n_sp, n_fs, wbuf, z_s, z_r, f_s, f_r)
+    here.wait()
+    start()
+    for w in range(count):
+        local[w].wait()
+        gather.send(w)
+    finish()
+
+    def norm(i, c):
+        at = pl.ds(pl.multiple_of(i * 16, 16), 16)
+        normbuf[at, :] = rms_rows(tokbuf[at, :], gain_ref[...])
+        return c
+
+    lax.fori_loop(0, tokbuf.shape[0] // 16, norm, 0)
+    pre_ref[...] = jnp.dot(normbuf[...], wbd_ref[...], preferred_element_type=jnp.float32)
+    depth = wbuf.shape[2]
+
+    def project(w):
+        total = None
+        for s in range(n_sp):
+            part = jnp.dot(normbuf[:, s * depth:(s + 1) * depth], wbuf[w, s], preferred_element_type=jnp.float32)
+            total = part if total is None else total + part
+        proj_ref[w] = total.astype(jnp.bfloat16)
+
+    for w in range(count):
+        gather.forward(w)
+        if w >= 1:
+            gather.finish(w - 1)
+            if w - 1 < count - 2:
+                project(w - 1)
+    gather.flush(count - 1)
+    gather.finish(count - 1)
+    out = pltpu.make_async_copy(wbuf.at[pl.ds(count - 2, 2)], wo_ref, loc.at[0])
+    out.start()
+    drain()
+    for w in range(count):
+        gather.drain(w)
+    out.wait()
+
+
+def project_call(n_sp, n_fs, n_tp, tokens, gain, w_bd, weights):
+    rows, width = tokens.shape
+    depth, cols = weights[0].shape
+    length = halo + n_tp * rows
+    count = len(weights)
+    slots = max(1, 2 ** len(share_bits(n_fs)) - 1)
+    hop = max(1, n_sp - 1)
+    dma = pltpu.SemaphoreType.DMA
+    vmem, anywhere = pl.BlockSpec(memory_space=pltpu.VMEM), pl.BlockSpec(memory_space=pl.ANY)
+    return pl.pallas_call(
+        functools.partial(project_kernel, n_sp, n_fs, n_tp),
+        out_shape=(
+            jax.ShapeDtypeStruct((count - 2, length, cols), jnp.bfloat16),
+            jax.ShapeDtypeStruct((length, w_bd.shape[1]), jnp.float32),
+            jax.ShapeDtypeStruct((2, n_sp, depth, cols), jnp.bfloat16),
+        ),
+        in_specs=[anywhere, vmem, vmem] + [anywhere] * count,
+        out_specs=(vmem, vmem, anywhere),
+        scratch_shapes=[
+            pltpu.VMEM((length, width), jnp.bfloat16),
+            pltpu.VMEM((length, width), jnp.bfloat16),
+            pltpu.VMEM((count, n_sp, depth, cols), jnp.bfloat16),
+            dma((count + 1,)), dma((max(1, n_tp - 1),)), dma((max(1, n_tp - 1),)), dma((n_tp,)), dma((n_tp,)),
+            dma((count, hop)), dma((count, hop)), dma((count, hop, slots)), dma((count, hop, slots)),
+        ],
+        compiler_params=pltpu.CompilerParams(collective_id=0, has_side_effects=True, vmem_limit_bytes=50 << 20),
+    )(tokens, gain, w_bd, *weights)
+
+
+def lower_inverse(corr, block):
+    at = jnp.arange(block)
+    done = jnp.broadcast_to(jnp.eye(block, dtype=jnp.float32), corr.shape)
+    size = 1
+    while size < block:
+        pair = (at[:, None] // (2 * size) == at[None, :] // (2 * size)) & (
+            at[:, None] // size != at[None, :] // size)
+        off = jnp.where(pair, corr, 0.0)
+        if size == 1:
+            done = done - off
+        else:
+            half = jnp.einsum("...ij,...jk->...ik", off, done, precision=highest)
+            done = done - jnp.einsum("...ij,...jk->...ik", done, half, precision=highest)
+        size *= 2
+    return done
 
 
 def from_behind(block, axis, distance):
@@ -49,13 +342,7 @@
         jnp.einsum("hnid,hnjd->hnij", key_scaled_beta, key_part, precision=highest) * decay_tab,
         0.0,
     )
-    identity = jnp.eye(block, dtype=jnp.float32)
-    inverse = lax.linalg.triangular_solve(
-        identity + corr_lower,
-        jnp.broadcast_to(identity, corr_lower.shape),
-        left_side=True,
-        lower=True,
-    )
+    inverse = lower_inverse(corr_lower, block)
     fixed_values = jnp.einsum("hnij,hnjd->hnid", inverse, value_beta, precision=highest)
     key_weights = jnp.einsum(
         "hnij,hnjd->hnid",
@@ -120,44 +407,27 @@
     w_out_pool,
     w_out_delta,
 ):
-    pool_w, query_w, key_w, value_w, gate_w, outp_w, outd_w = (
-        lax.all_gather(w_pool_in, "sp", axis=0, tiled=True),
-        lax.all_gather(w_query, "sp", axis=0, tiled=True),
-        lax.all_gather(w_key, "sp", axis=0, tiled=True),
-        lax.all_gather(w_value, "sp", axis=0, tiled=True),
-        lax.all_gather(w_gate, "sp", axis=0, tiled=True),
-        lax.all_gather(w_out_pool, "sp", axis=1, tiled=True),
-        lax.all_gather(w_out_delta, "sp", axis=1, tiled=True),
-    )
-    rows_all = lax.all_gather(tokens, "tp", axis=0, tiled=True)
-    norm_result = rms_rows(rows_all, norm_gain)
-    length = norm_result.shape[0]
-
-    def project(weight):
-        return jnp.dot(norm_result, weight, preferred_element_type=jnp.float32).astype(jnp.bfloat16)
-
-    pool_in = project(pool_w)
-    query_raw = project(query_w)
-    key_raw = project(key_w)
-    value_raw = project(value_w)
-    gate_raw = project(gate_w)
+    n_sp, n_fs, n_tp = (lax.axis_size(a) for a in ("sp", "fs", "tp"))
+    proj, both_pre, gathered_out = project_call(
+        n_sp, n_fs, n_tp, tokens, norm_gain.reshape(1, -1), jnp.concatenate([w_beta, w_decay], axis=1),
+        (w_key, w_query, w_value, w_gate, w_pool_in, w_out_pool, w_out_delta))
+    both_pre = both_pre[halo:]
+    before = proj[:, halo - tail_rows:halo]
+    key_raw, query_raw, value_raw, gate_raw, pool_in = (proj[i, halo:] for i in range(5))
+    length = pool_in.shape[0]
+    outp_w, outd_w = (
+        jnp.transpose(gathered_out[i], (1, 0, 2)).reshape(w_out_pool.shape[0], -1) for i in range(2))
     heads_dev = a_log.shape[0]
     head_dim = query_raw.shape[1] // heads_dev
     width_dev = heads_dev * head_dim
     all_heads = w_beta.shape[1]
     lane = lax.axis_index("tp")
-    both_pre = jnp.dot(
-        norm_result, jnp.concatenate([w_beta, w_decay], axis=1), preferred_element_type=jnp.float32
-    )
     beta_pre = lax.dynamic_slice_in_dim(both_pre[:, :all_heads], lane * heads_dev, heads_dev, 1)
     forget_logits = lax.dynamic_slice_in_dim(
         both_pre[:, all_heads:], lane * heads_dev, heads_dev, 1
     )
     raw_three = jnp.concatenate([query_raw, key_raw, value_raw], axis=1)
-    tails = jnp.concatenate(
-        [pool_in[length - tail_rows :], raw_three[length - tail_rows :]], axis=1
-    )
-    prior_state = from_behind(tails, "sp", 1)
+    prior_state = jnp.concatenate([before[4], before[1], before[0], before[2]], axis=1)
     pool_width_dev = pool_in.shape[1]
     source_rows = pool_in.astype(jnp.float32)
     extended = jnp.concatenate(

time: 435 us -> 251 us (0.58)
  waiting for transfers between devices: 274 us -> 37.2 us
  Pallas kernels: 0 us -> 106 us
  other arithmetic: 87.7 us -> 18.5 us
  local copies, waits for them, and re-layouts: 2.05 us -> 26.3 us
  matrix products: 48.3 us -> 39.8 us
    all_gather x8 -> x0, waiting for transfers between devices: 231 us -> none  [the longest x1 43.6 us: per_device(): lax.all_gather(w_query, 'sp', axis=0, tiled=True)]
    pallas_call x0 -> x1, Pallas kernels: none -> 106 us  [project_call(): pl.pallas_call(functools.partial(project_kernel, n_sp, n_fs, n_tp), out_s...]
    another operation x5 -> x3, other arithmetic: 79.6 us -> 0.76 us  [the longest x1 78.8 us: block_terms(): lax.linalg.triangular_solve(identity + corr_lower, jnp.broadcast_to(ident...]
    unnamed x33 -> x87, local copies, waits for them, and re-layouts: 0.84 us -> 9.68 us
    dot_general x6 -> x10, matrix products: 14.9 us -> 6.59 us  [the longest x5 3.33 us: lower_inverse(): half = jnp.einsum('...ij,...jk->...ik', off, done, precision=highest)]
    transpose x0 -> x4, local copies, waits for them, and re-layouts: none -> 6.98 us  [the longest x3 6.8 us: per_device(): jnp.transpose(gathered_out[i], (1, 0, 2)).reshape(w_out_pool.shape[0], -1)]
    unnamed x9 -> x1, waiting for transfers between devices: 5.07 us -> 0.02 us
    ppermute x4 -> x3, waiting for transfers between devices: 13.9 us -> 15.2 us  [from_behind(): return lax.ppermute(block, axis, route)]
  transfers between devices with their start and end apart: 13 -> 4, of which waited for: 10 -> 4; matrix products, arithmetic and copies ran while one was open for 31% -> 0% of each run, Pallas kernels for 0% -> 0%
where the time goes in v1:
time: 251 us; the launch traced here: 246 us
  Pallas kernels  106 us (42%)
  matrix products  39.8 us (16%)
  waiting for transfers between devices  37.2 us (15%)
  local copies, waits for them, and re-layouts  26.3 us (10%)
  other arithmetic  18.5 us (7%)
  between operations  14.4 us (6%)
  starting transfers between devices  3.88 us (2%)
    pallas_call x1, Pallas kernels, project_call(): pl.pallas_call(functools.partial(project_kernel, n_sp, n_fs, n_tp), out_s...  106 us
    reduce_scatter x1, waiting for transfers between devices, per_device(): lax.psum_scatter(lax.optimization_barrier(value_partial_rows.astype(jnp.b...  22 us
    ppermute x3, waiting for transfers between devices, from_behind(): return lax.ppermute(block, axis, route)  15.2 us
    unnamed x87, local copies, waits for them, and re-layouts  9.68 us
    transpose x3, local copies, waits for them, and re-layouts, per_device(): jnp.transpose(gathered_out[i], (1, 0, 2)).reshape(w_out_pool.shape[0], -1)  6.8 us
    dot_general x4, matrix products, compose_step(): jnp.einsum('hcd,hce->hde', key_decayed, fresh, precision=highest)  5.14 us
  transfers between devices with their start and end apart: 4, of which 4 were waited for; matrix products, arithmetic and copies ran while one was open for 0% of the time, Pallas kernels for 0%

profile of v1, /device:TPU:31, one launch (start us, length us, event | category | flops | bytes accessed | tf_op | source)
XLA Modules:
  0.0 246.4 jit_solution(18054934582633391545)
XLA Ops:
  6.5 0.7 reshape.628.refs_1_
  7.3 0.8 pad_maximum_fusion.2
  8.3 1.0 copy-done.1
  9.4 1.0 copy-done.2
  10.4 1.0 copy-done.3
  11.5 1.0 copy-done.4
  12.5 1.0 copy-done.5
  13.5 1.0 copy-done.6
  14.6 105.8 %shard_map.163 = (bf16[5,272,512]{2,1,0:T(8,128)(2,1)}, f32[272,16]{1,0:T(8,128)S(1)}, bf16[2,4,512,512]{3,2,1,0:T(8,128)(2,1)}) custom-call(bf16[128,2048]{1,0:T(8,128)(2,1)S(1)} %copy-done.1, bf16[1,2048]{1,0:T(2,128)(2,1)S(1)} %reshape.628.refs_1_, bf16[2048,16]{1,0:T(8,128)(2,1)S(1)} %copy.139.refs_2_, bf16[512,512]{1,0:T(8,128)(2,1)S(1)} %copy-done.2, ...), custom_call_target="tpu_custom_call" | custom-call | tf_op jit(solution)/shard_map/pallas_call | solution.py:271
  120.4 2.3 slice_convert_fusion
  122.7 1.4 slice_bitcast_fusion.10
  131.1 0.8 slice.159
  132.2 1.1 copy-done.8
  133.3 1.6 slice_bitcast_fusion
  134.9 2.4 copy.144
  138.0 1.1 reduce_window_sum.28
  139.3 0.7 fusion.132
  139.9 0.7 copy.153
  140.6 1.0 slice_reduce_fusion.4
  141.9 0.9 divide_multiply_fusion
  142.8 1.0 slice_bitcast_fusion.2
  144.1 1.0 fusion.61
  145.6 1.0 fusion.45
  146.8 0.7 fusion.89
  147.5 0.7 convolution_subtract_fusion.7
  153.5 0.9 convolution_bitcast_fusion.2
  154.6 0.7 convolution_bitcast_fusion.1
  155.6 13.5 %while.37 = (s32[]{:T(128)}, f32[4,128,128]{2,1,0:T(8,128)S(1)}, f32[4,128,128]{2,1,0:T(8,128)S(1)}, f32[4,4]{1,0:T(4,128)}, f32[4,4,64,128]{3,2,1,0:T(8,128)S(1...) while((s32[]{:T(128)}, f32[4,128,128]{2,1,0:T(8,128)S(1)}, ...), condition=%wide.region_5.6_spmd.clone, body=%wide.region_4.5_spmd.clone.sunk | while | flops 201752576 | bytes 2754827 | solution.py:481
  156.0 0.7 fusion.209
  157.7 1.3 convolution_add_fusion.8
  159.4 0.7 fusion.209
  161.1 1.3 convolution_add_fusion.8
  162.7 0.7 fusion.209
  164.5 1.3 convolution_add_fusion.8
  166.1 0.7 fusion.209
  167.8 1.3 convolution_add_fusion.8
  169.1 0.7 add_rsqrt_fusion.1
  170.3 1.8 fusion.47
  172.1 20.4 %while.38 = (s32[]{:T(128)}, f32[4,128,128]{2,1,0:T(8,128)S(1)}, f32[4,128,128]{2,1,0:T(8,128)S(1)}, f32[4,128,128]{2,1,0:T(8,128)S(1)}, s32[]{:T(128)}, /*index=5*/s32[]{:T(128)}) while((s32[]{:T(128)}, f32[4,128,128]{2,1,0:T(8,128)S(1)}, f32[4,128,128]{2,1,0:T(8,128)S(1)}, f32[4,128,128]{2,1,0:T(8,128)S(1)}, s32[]{:T(128)}, ...), condition=%wide.region_7.8_spmd.clone, body=%wide.region_6.7_spmd.clone.sunk | while | flops 100925440 | bytes 1835127 | solution.py:488
  172.5 1.3 collective-permute-start
  173.8 5.4 %collective-permute-done = bf16[4,128,128]{2,1,0:T(8,128)(2,1)S(1)} collective-permute-done((bf16[4,128,128]{2,1,0:T(8,128)(2,1)S(1)}, bf16[4,128,128]{2,1,0:T(8,128)(2,1)S(1)}, u32[]{:S(2)}, u32[]{:S(2)}) %collective-permute-start) | collective-permute-done | bytes 131104 | tf_op jit(solution)/shard_map/while/body/eval_jaxpr/ppermute | solution.py:311
  179.7 1.3 collective-permute-start
  181.0 5.3 %collective-permute-done = bf16[4,128,128]{2,1,0:T(8,128)(2,1)S(1)} collective-permute-done((bf16[4,128,128]{2,1,0:T(8,128)(2,1)S(1)}, bf16[4,128,128]{2,1,0:T(8,128)(2,1)S(1)}, u32[]{:S(2)}, u32[]{:S(2)}) %collective-permute-start) | collective-permute-done | bytes 131104 | tf_op jit(solution)/shard_map/while/body/eval_jaxpr/ppermute | solution.py:311
  186.7 1.3 collective-permute-start
  188.0 4.4 %collective-permute-done = bf16[4,128,128]{2,1,0:T(8,128)(2,1)S(1)} collective-permute-done((bf16[4,128,128]{2,1,0:T(8,128)(2,1)S(1)}, bf16[4,128,128]{2,1,0:T(8,128)(2,1)S(1)}, u32[]{:S(2)}, u32[]{:S(2)}) %collective-permute-start) | collective-permute-done | bytes 131104 | tf_op jit(solution)/shard_map/while/body/eval_jaxpr/ppermute | solution.py:311
  192.5 15.6 %while.36 = (s32[]{:T(128)}, f32[4,128,128]{2,1,0:T(8,128)S(1)}, f32[4,4,64,128]{3,2,0,1:T(8,128)}, f32[4,4]{1,0:T(4,128)}, f32[4,4,64,128]{3,2,1,0:T(8,128)S(1)...) while((s32[]{:T(128)}, f32[4,128,128]{2,1,0:T(8,128)S(1)}, ...), condition=%wide.region_10.11_spmd, body=%wide.region_9.10_spmd.sunk | while | flops 176357376 | bytes 2493081 | solution.py:489
  192.9 1.2 fusion.198
  194.0 1.0 fusion.199
  195.1 0.7 fusion.197
  196.8 1.2 fusion.198
  197.9 1.0 fusion.199
  199.0 0.7 fusion.197
  200.7 1.2 fusion.198
  201.8 1.0 fusion.199
  202.9 0.7 fusion.197
  204.6 1.2 fusion.198
  205.7 1.0 fusion.199
  206.8 0.7 fusion.197
  208.3 1.3 fusion.77
  210.1 2.8 %copy.170 = bf16[512,4,512]{0,2,1:T(8,128)(2,1)S(1)} copy(bf16[512,4,512]{2,0,1:T(8,128)(2,1)} %get-tuple-element.285) | data formatting | bytes 4194304 | tf_op jit(solution)/shard_map/transpose | solution.py:419
  213.1 1.9 fusion.48
  215.0 0.8 fusion.133
  215.8 1.8 fusion.41
  217.5 22.0 %reduce-scatter.2.cloned.1.call-done = bf16[128,2048]{1,0:T(8,128)(2,1)} async-done(((bf16[256,2048]{1,0:T(8,128)(2,1)}), bf16[128,2048]{1,0:T(8,128)(2,1)}) %reduce-scatter.2.cloned.1.call-update) | async-done | bytes 524304 | tf_op jit(solution)/shard_map/reduce_scatter | solution.py:501
  (172 shorter events, 26.6 us)
Async XLA Ops:
  6.5 206.4 %copy-start = (bf16[4,128,128]{2,1,0:T(8,128)(2,1)S(1)}, bf16[4,128,128]{2,1,0:T(8,128)(2,1)}, u32[]{:S(2)}) copy-start(bf16[4,128,128]{2,1,0:T(8,128)(2,1)} %param.35) | copy-start | bytes 393220
  6.5 233.0 %reduce-scatter.2.cloned.1.call-start = ((), (), s32[]{:S(2)}) async-start(), calls=%async_computation.1 | async-start | bytes 1572864 | tf_op jit(solution)/shard_map/reduce_scatter | solution.py:501
  8.3 1.0 copy-start.1
  9.4 1.0 copy-start.2
  10.4 1.0 copy-start.3
  11.5 1.0 copy-start.4
  12.5 1.0 copy-start.5
  13.5 1.0 copy-start.6
  130.7 2.7 %copy-start.8 = (bf16[2,4,512,512]{3,2,1,0:T(8,128)(2,1)S(1)}, bf16[2,4,512,512]{3,2,1,0:T(8,128)(2,1)}, u32[]{:S(2)}) copy-start(bf16[2,4,512,512]{3,2,1,0:T(8,128)(2,1)} %get-tuple-element.116) | copy-start | bytes 12582916
  131.1 1.1 copy-start.9
  134.9 2.8 %copy-start.36 = (f32[4]{0:T(128)S(1)}, f32[4]{0:T(128)}, u32[]{:S(2)}) copy-start(f32[4]{0:T(128)} %param.33) | copy-start | bytes 52
  134.9 2.8 %copy-start.25 = (f32[256,4]{0,1:T(4,128)S(1)}, f32[256,4]{0,1:T(4,128)}, u32[]{:S(2)}) copy-start(f32[256,4]{0,1:T(4,128)} %param.34) | copy-start | bytes 12292
  137.3 4.3 %copy-start.14 = (bf16[256,512]{1,0:T(8,128)(2,1)S(1)}, bf16[256,512]{1,0:T(8,128)(2,1)}, u32[]{:S(2)}) copy-start(bf16[256,512]{1,0:T(8,128)(2,1)} %get-tuple-element.293) | copy-start | bytes 786436
  137.3 4.4 %copy-start.20 = (bf16[15,512]{1,0:T(8,128)(2,1)S(1)}, bf16[15,512]{1,0:T(8,128)(2,1)}, u32[]{:S(2)}) copy-start(bf16[15,512]{1,0:T(8,128)(2,1)} %get-tuple-element.295) | copy-start | bytes 46084
  137.3 4.4 %copy-start.21 = (bf16[15,512]{1,0:T(8,128)(2,1)S(1)}, bf16[15,512]{1,0:T(8,128)(2,1)}, u32[]{:S(2)}) copy-start(bf16[15,512]{1,0:T(8,128)(2,1)} %get-tuple-element.296) | copy-start | bytes 46084
  137.3 4.4 %copy-start.22 = (bf16[15,512]{1,0:T(8,128)(2,1)S(1)}, bf16[15,512]{1,0:T(8,128)(2,1)}, u32[]{:S(2)}) copy-start(bf16[15,512]{1,0:T(8,128)(2,1)} %get-tuple-element.297) | copy-start | bytes 46084
  143.9 1.2 copy-start.24
  144.1 1.4 copy-start.34
  145.3 1.4 copy-start.26
  145.3 1.4 copy-start.27
  145.3 1.4 copy-start.28
  145.3 1.4 copy-start.29
  145.3 1.4 copy-start.30
  145.3 1.4 copy-start.31
  145.3 1.5 copy-start.15
  145.6 1.1 copy-start.18
  152.2 1.3 copy-start.17
  153.5 1.0 copy-start.13
  154.5 0.8 copy-start.16
  156.7 0.6 copy-start.23
  160.1 0.6 copy-start.23
  163.4 0.6 copy-start.23
  166.8 0.6 copy-start.23
  169.1 1.1 copy-start.19
  172.5 6.7 %collective-permute-start = (bf16[4,128,128]{2,1,0:T(8,128)(2,1)S(1)}, bf16[4,128,128]{2,1,0:T(8,128)(2,1)S(1)}, u32[]{:S(2)}, u32[]{:S(2)}) collective-permute-start(bf16[4,128,128]{2,1,0:T(8,128)(2,1)S(1)} %fusion.212), channel_id=1, source_target_pairs={{0,8},{8,16},{16,24},{1,9},{9,17},{17,25},{2,10},{10,18},{18,26},{... | collective-permute-start | bytes 393224 | tf_op jit(solution)/shard_map/while/body/eval_jaxpr/ppermute | solution.py:311
  179.7 6.6 %collective-permute-start = (bf16[4,128,128]{2,1,0:T(8,128)(2,1)S(1)}, bf16[4,128,128]{2,1,0:T(8,128)(2,1)S(1)}, u32[]{:S(2)}, u32[]{:S(2)}) collective-permute-start(bf16[4,128,128]{2,1,0:T(8,128)(2,1)S(1)} %fusion.212), channel_id=1, source_target_pairs={{0,8},{8,16},{16,24},{1,9},{9,17},{17,25},{2,10},{10,18},{18,26},{... | collective-permute-start | bytes 393224 | tf_op jit(solution)/shard_map/while/body/eval_jaxpr/ppermute | solution.py:311
  186.7 5.7 %collective-permute-start = (bf16[4,128,128]{2,1,0:T(8,128)(2,1)S(1)}, bf16[4,128,128]{2,1,0:T(8,128)(2,1)S(1)}, u32[]{:S(2)}, u32[]{:S(2)}) collective-permute-start(bf16[4,128,128]{2,1,0:T(8,128)(2,1)S(1)} %fusion.212), channel_id=1, source_target_pairs={{0,8},{8,16},{16,24},{1,9},{9,17},{17,25},{2,10},{10,18},{18,26},{... | collective-permute-start | bytes 393224 | tf_op jit(solution)/shard_map/while/body/eval_jaxpr/ppermute | solution.py:311
  192.5 15.6 %copy-start.12 = (f32[1,256,512]{2,1,0:T(8,128)S(1)}, f32[1,256,512]{2,1,0:T(8,128)}, u32[]{:S(2)}) copy-start(f32[1,256,512]{2,1,0:T(8,128)} %get-tuple-element.290) | copy-start | bytes 1572868
  192.5 17.2 %copy-start.33 = (f32[128]{0:T(128)S(1)}, f32[128]{0:T(128)}, u32[]{:S(2)}) copy-start(f32[128]{0:T(128)} %param.37) | copy-start | bytes 1540
  208.1 1.6 copy-start.11
  210.0 3.0 %copy-start.10 = (f32[512,3,128]{0,2,1:T(8,128)S(1)}, f32[512,3,128]{0,2,1:T(8,128)}, u32[]{:S(2)}) copy-start(f32[512,3,128]{0,2,1:T(8,128)} %copy-done.9) | copy-start | bytes 2359300
  210.0 3.0 %copy-start.32 = (s32[512]{0:T(512)S(1)}, s32[512]{0:T(512)}, u32[]{:S(2)}) copy-start(s32[512]{0:T(512)} %fusion.120) | copy-start | bytes 6148
  210.1 3.0 %copy-start.35 = (f32[512]{0:T(512)S(1)}, f32[512]{0:T(512)}, u32[]{:S(2)}) copy-start(f32[512]{0:T(512)} %param.36) | copy-start | bytes 6148
  210.1 2.9 %copy-start.37 = (s32[256]{0:T(256)S(1)}, s32[256]{0:T(256)}, u32[]{:S(2)}) copy-start(s32[256]{0:T(256)} %add_add_fusion) | copy-start | bytes 3076
  210.1 2.9 %copy-start.38 = (pred[512]{0:T(512)(128)(4,1)S(1)}, pred[512]{0:T(512)(128)(4,1)}, u32[]{:S(2)}) copy-start(pred[512]{0:T(512)(128)(4,1)} %get-tuple-element.309) | copy-start | bytes 1540
  210.1 2.9 %copy-start.39 = (pred[512]{0:T(512)(128)(4,1)S(1)}, pred[512]{0:T(512)(128)(4,1)}, u32[]{:S(2)}) copy-start(pred[512]{0:T(512)(128)(4,1)} %get-tuple-element.310) | copy-start | bytes 1540
  210.1 2.9 %copy-start.40 = (pred[512]{0:T(512)(128)(4,1)S(1)}, pred[512]{0:T(512)(128)(4,1)}, u32[]{:S(2)}) copy-start(pred[512]{0:T(512)(128)(4,1)} %get-tuple-element.311) | copy-start | bytes 1540
  210.1 2.9 %copy-start.41 = (pred[512]{0:T(512)(128)(4,1)S(1)}, pred[512]{0:T(512)(128)(4,1)}, u32[]{:S(2)}) copy-start(pred[512]{0:T(512)(128)(4,1)} %get-tuple-element.312) | copy-start | bytes 1540
  213.1 1.9 copy-start.7
Sparse Core Ops, SparseCore 0:
  217.7 21.8 reduce-scatter.1

commit v2 on v1

v2 whole, which is shorter than its diff:
```python
import functools

import jax
import jax.numpy as jnp
from jax import lax
from jax.experimental import pallas as pl
from jax.experimental.pallas import tpu as pltpu
from jax.sharding import PartitionSpec as P

BLOCK = 64
PAIR = 2 * BLOCK

eps = 1e-06
halo = 16
MESH = pl.DeviceIdType.MESH
highest = lax.Precision.HIGHEST
f32 = jnp.float32
bf16 = jnp.bfloat16
KEY, QUERY, VALUE, POOL, GATE, OUT_POOL, OUT_DELTA = range(7)
AHEAD = 1


def mm(a, b, dims=((1,), (0,)), precision=highest):
    return lax.dot_general(a, b, (dims, ((), ())), precision=precision, preferred_element_type=f32)


def rms_rows(values, gain):
    floats = values.astype(f32)
    scale = lax.rsqrt(jnp.mean(floats * floats, axis=-1, keepdims=True) + eps)
    return (floats * scale * gain.astype(f32)).astype(bf16)


def unit_rows(values):
    return values * lax.rsqrt(jnp.sum(values * values, axis=-1, keepdims=True) + eps)


def silu(x):
    return x * jax.nn.sigmoid(x)


def share_bits(n_fs):
    if n_fs & (n_fs - 1):
        return []
    return [n_fs >> (k + 1) for k in range(n_fs.bit_length() - 1)]


class Gather:
    def __init__(self, n_sp, n_fs, wbuf, z_s, z_r, f_s, f_r):
        self.n_sp, self.bits = n_sp, share_bits(n_fs)
        self.wbuf, self.z_s, self.z_r, self.f_s, self.f_r = wbuf, z_s, z_r, f_s, f_r
        self.sp, self.fs = lax.axis_index("sp"), lax.axis_index("fs")
        self.pieces = 2 ** len(self.bits)
        self.mine = self.fs if self.bits else 0 * self.fs
        self.depth = wbuf.shape[2] // self.pieces

    def partner(self, bit):
        return self.fs + bit * (1 - 2 * (self.fs // bit % 2))

    def mask_of(self, m, index):
        for i, bit in enumerate(self.bits):
            if m >> i & 1:
                index = index + bit * (1 - 2 * (index // bit % 2))
        return index

    def piece(self, w, src, index):
        return self.wbuf.at[w, src, pl.ds(pl.multiple_of(index * self.depth, self.depth), self.depth)]

    def z_copy(self, w, src, way):
        ref = self.piece(w, src, self.mine)
        to = lax.rem(self.sp + way + self.n_sp, self.n_sp)
        return pltpu.make_async_remote_copy(
            src_ref=ref, dst_ref=ref, send_sem=self.z_s.at[w, src, (way + 1) // 2], recv_sem=self.z_r.at[w, src],
            device_id={"sp": to}, device_id_type=MESH)

    def f_copy(self, w, src, k, m):
        slot = 2 ** k - 1 + m
        ref = self.piece(w, src, self.mask_of(m, self.mine))
        return pltpu.make_async_remote_copy(
            src_ref=ref, dst_ref=ref, send_sem=self.f_s.at[w, src, slot], recv_sem=self.f_r.at[w, src, slot],
            device_id={"fs": self.partner(self.bits[k])}, device_id_type=MESH)

    def can_send(self, way):
        return self.sp < self.n_sp - 1 if way == 1 else self.sp > 0

    def send(self, w):
        for way in (1, -1):
            @pl.when(self.can_send(way))
            def _():
                self.z_copy(w, self.sp, way).start()

    def each(self, t, act):
        for way in (1, -1):
            src = self.sp - way * t
            @pl.when(src >= 0 if way == 1 else src < self.n_sp)
            def _():
                act(src, way)

    def arrive_z(self, w, src, way):
        self.z_copy(w, src, way).wait_recv()

        @pl.when(self.can_send(way))
        def _():
            self.z_copy(w, src, way).start()
        for k in range(len(self.bits)):
            self.f_copy(w, src, k, 0).start()

    def arrive_f(self, w, t, k):
        def act(src, way):
            for m in range(2 ** k):
                self.f_copy(w, src, k, m).wait_recv()
                for later in range(k + 1, len(self.bits)):
                    self.f_copy(w, src, later, m | 1 << k).start()
        self.each(t, act)

    def forward(self, w):
        last = self.n_sp - 1
        inner = len(self.bits) - 1
        if w + AHEAD < self.wbuf.shape[0]:
            self.send(w + AHEAD)

        def body(t, c):
            self.each(t, lambda src, way: self.arrive_z(w, src, way))
            for k in range(inner):
                @pl.when(t > 1)
                def _():
                    self.arrive_f(w, t - 1, k)
                if w > 0:
                    @pl.when(t == 1)
                    def _():
                        self.arrive_f(w - 1, last, k)
            return c
        lax.fori_loop(1, self.n_sp, body, 0)

    def flush(self, w):
        for k in range(len(self.bits) - 1):
            self.arrive_f(w, self.n_sp - 1, k)

    def finish(self, w):
        if self.bits:
            def body(t, c):
                self.arrive_f(w, t, len(self.bits) - 1)
                return c
            lax.fori_loop(1, self.n_sp, body, 0)

    def drain(self, w):
        for way in (1, -1):
            @pl.when(self.can_send(way))
            def _():
                self.z_copy(w, self.sp, way).wait_send()

        def act(src, way):
            @pl.when(self.can_send(way))
            def _():
                self.z_copy(w, src, way).wait_send()
            for k in range(len(self.bits)):
                for m in range(2 ** k):
                    self.f_copy(w, src, k, m).wait_send()

        def body(t, c):
            self.each(t, act)
            return c
        lax.fori_loop(1, self.n_sp, body, 0)


def enter(n_sp, n_fs, n_tp):
    sp, fs, tp = (lax.axis_index(a) for a in ("sp", "fs", "tp"))
    barrier = pltpu.get_barrier_semaphore()
    bits = share_bits(n_fs)
    for d in range(1, n_sp):
        pl.semaphore_signal(barrier, inc=1, device_id={"sp": lax.rem(sp + d, n_sp)}, device_id_type=MESH)
    for bit in bits:
        pl.semaphore_signal(barrier, inc=1, device_id={"fs": fs + bit * (1 - 2 * (fs // bit % 2))}, device_id_type=MESH)
    for d in range(1, n_tp):
        pl.semaphore_signal(barrier, inc=1, device_id={"tp": lax.rem(tp + d, n_tp)}, device_id_type=MESH)
    pl.semaphore_wait(barrier, n_sp - 1 + len(bits) + n_tp - 1)


def gather_tokens(n_sp, n_tp, tokbuf, rows, tok_s, tok_r, halo_s, halo_r):
    sp, tp = lax.axis_index("sp"), lax.axis_index("tp")

    def tok_copy(d, owner):
        ref = tokbuf.at[pl.ds(pl.multiple_of(halo + owner * rows, 16), rows)]
        return pltpu.make_async_remote_copy(
            src_ref=ref, dst_ref=ref, send_sem=tok_s.at[d - 1], recv_sem=tok_r.at[d - 1],
            device_id={"tp": lax.rem(tp + d, n_tp)}, device_id_type=MESH)

    def halo_next():
        return pltpu.make_async_remote_copy(
            src_ref=tokbuf.at[pl.ds(n_tp * rows, halo)], dst_ref=tokbuf.at[pl.ds(0, halo)],
            send_sem=halo_s.at[0], recv_sem=halo_r.at[0],
            device_id={"sp": lax.rem(sp + 1, n_sp)}, device_id_type=MESH)

    def halo_side(d):
        ref = tokbuf.at[pl.ds(0, halo)]
        return pltpu.make_async_remote_copy(
            src_ref=ref, dst_ref=ref, send_sem=halo_s.at[d], recv_sem=halo_r.at[d],
            device_id={"tp": lax.rem(tp + d, n_tp)}, device_id_type=MESH)

    end = n_tp - 1

    def start():
        for d in range(1, n_tp):
            tok_copy(d, tp).start()

        @pl.when(jnp.logical_and(tp == end, sp < n_sp - 1))
        def _():
            halo_next().start()

        @pl.when(sp == 0)
        def _():
            tokbuf[0:halo, :] = jnp.zeros((halo, tokbuf.shape[1]), tokbuf.dtype)

    def finish():
        @pl.when(jnp.logical_and(tp == end, sp > 0))
        def _():
            halo_next().wait_recv()
            for d in range(1, n_tp):
                halo_side(d).start()
        for d in range(1, n_tp):
            tok_copy(d, lax.rem(tp - d + n_tp, n_tp)).wait_recv()

        @pl.when(jnp.logical_and(tp < end, sp > 0))
        def _():
            for d in range(1, n_tp):
                @pl.when(tp == d - 1)
                def _():
                    halo_side(d).wait_recv()

    def drain():
        for d in range(1, n_tp):
            tok_copy(d, tp).wait_send()

        @pl.when(jnp.logical_and(tp == end, sp < n_sp - 1))
        def _():
            halo_next().wait_send()

        @pl.when(jnp.logical_and(tp == end, sp > 0))
        def _():
            for d in range(1, n_tp):
                halo_side(d).wait_send()

    return start, finish, drain


def mixer_kernel(n_sp, n_fs, n_tp, *refs):
    tok_ref, gain_ref, wbd_ref, conv_ref, alog_ref, extra_ref, mix_ref, scale_ref, dgain_ref = refs[:9]
    w_refs = refs[9:16]
    out_ref = refs[16]
    (tokbuf, normbuf, wbuf, raw, pool_out, delta_out, pbuf, cbuf, s_in, s_out, part, rsbuf,
     loc, tok_s, tok_r, halo_s, halo_r, z_s, z_r, f_s, f_r, st_s, st_r, rs_s, rs_r) = refs[17:]
    rows, width = tok_ref.shape
    length = n_tp * rows
    heads, head_dim = cbuf.shape[0], cbuf.shape[1]
    groups, group_dim = mix_ref.shape[0], mix_ref.shape[1]
    sp, tp = lax.axis_index("sp"), lax.axis_index("tp")
    count = len(w_refs)
    local = [pltpu.make_async_copy(w_refs[i], wbuf.at[i, sp], loc.at[i]) for i in range(count)]
    here = pltpu.make_async_copy(
        tok_ref, tokbuf.at[pl.ds(pl.multiple_of(halo + tp * rows, 16), rows)], loc.at[count])
    here.start()
    for copy in local:
        copy.start()
    enter(n_sp, n_fs, n_tp)
    start, finish, drain = gather_tokens(n_sp, n_tp, tokbuf, rows, tok_s, tok_r, halo_s, halo_r)
    gather = Gather(n_sp, n_fs, wbuf, z_s, z_r, f_s, f_r)
    here.wait()
    start()
    for w in range(count):
        local[w].wait()
        if w < AHEAD:
            gather.send(w)
    depth = wbuf.shape[2]

    def norm(i, c):
        at = pl.ds(pl.multiple_of(i * 16, 16), 16)
        normbuf[at, :] = rms_rows(tokbuf[at, :], gain_ref[...])
        return c

    def project(w):
        total = None
        for s in range(n_sp):
            term = jnp.dot(normbuf[:, s * depth:(s + 1) * depth], wbuf[w, s], preferred_element_type=f32)
            total = term if total is None else total + term
        raw[w] = total.astype(bf16).astype(f32)

    gather.forward(0)
    finish()
    lax.fori_loop(0, tokbuf.shape[0] // 16, norm, 0)
    pre = jnp.dot(normbuf[...], wbd_ref[...], preferred_element_type=f32)[halo:]
    softplus = jnp.maximum(pre, 0.0) + jnp.log1p(jnp.exp(-jnp.abs(pre)))
    log_gate = -jnp.exp(alog_ref[...]) * softplus + extra_ref[...]
    strength = jax.nn.sigmoid(pre)
    row = lax.broadcasted_iota(jnp.int32, (length, length), 0)
    col = lax.broadcasted_iota(jnp.int32, (length, length), 1)
    tri = jnp.where((row // BLOCK == col // BLOCK) & (row >= col), 1.0, 0.0)
    cum = mm(tri, log_gate)
    cum_t = cum.T

    gather.forward(1)
    gather.finish(0)
    project(0)
    gather.forward(2)
    gather.finish(1)
    project(1)
    gather.forward(3)
    gather.finish(2)
    project(2)

    def active(role, w, h):
        at = slice(h * head_dim, (h + 1) * head_dim)
        taps = conv_ref.shape[1]
        total = None
        for j in range(taps):
            term = raw[w, pl.ds(halo - (taps - 1) + j, length), at] * conv_ref[role, j:j + 1, at]
            total = term if total is None else total + term
        return silu(total)

    unit = min(PAIR, length)
    i2 = lax.broadcasted_iota(jnp.int32, (unit, unit), 0)
    j2 = lax.broadcasted_iota(jnp.int32, (unit, unit), 1)
    lower = (i2 // BLOCK == j2 // BLOCK) & (i2 >= j2)
    strict = lower & (i2 > j2)
    eye = jnp.where(i2 == j2, 1.0, 0.0)

    def delta(some):
        units = []
        for h in some:
            q = unit_rows(active(0, QUERY, h)) * head_dim ** (-0.5)
            k = unit_rows(active(1, KEY, h))
            v = active(2, VALUE, h)
            beta = strength[:, heads + h:heads + h + 1]
            g = cum[:, h:h + 1]
            grow = jnp.exp(g)
            kb = k * beta
            right = jnp.concatenate([v * beta, kb * grow], axis=1)
            qg = q * grow
            for p in range(length // unit):
                at = slice(p * unit, (p + 1) * unit)
                gaps = g[at] - cum_t[h:h + 1, at]
                decay = jnp.where(lower, jnp.exp(jnp.where(lower, gaps, 0.0)), 0.0)
                both = mm(jnp.concatenate([kb[at], q[at]], axis=0), k[at], ((1,), (1,)))
                corr = jnp.where(strict, both[:unit] * decay, 0.0)
                scores = both[unit:] * decay
                units.append([h, p, corr, scores, right[at], qg[at], k[at], g[at]])
        done = [eye - jnp.where((i2 // 2 == j2 // 2), u[2], 0.0) for u in units]
        size = 2
        while size < BLOCK:
            pair = (i2 // (2 * size) == j2 // (2 * size)) & (i2 // size != j2 // size)
            half = [mm(jnp.where(pair, u[2], 0.0), x) for u, x in zip(units, done)]
            done = [x - mm(x, y) for x, y in zip(done, half)]
            size *= 2
        solved = [mm(x, u[4]) for u, x in zip(units, done)]
        carry = {h: jnp.concatenate([jnp.where(
            lax.broadcasted_iota(jnp.int32, (head_dim, head_dim), 0)
            == lax.broadcasted_iota(jnp.int32, (head_dim, head_dim), 1), 1.0, 0.0),
            jnp.zeros((head_dim, head_dim), f32)], axis=1) for h in some}
        per = length // unit
        for p in range(per):
            for b in range(unit // BLOCK):
                at = slice(b * BLOCK, (b + 1) * BLOCK)
                for n, h in enumerate(some):
                    _, _, _, scores, _, qg, k, g = units[n * per + p]
                    fixed = solved[n * per + p][at, :head_dim]
                    kw = solved[n * per + p][at, head_dim:]
                    last = g[(b + 1) * BLOCK - 1:(b + 1) * BLOCK]
                    fall = k[at] * jnp.exp(last - g[at])
                    c = carry[h]
                    two = mm(jnp.concatenate([kw, qg[at]], axis=0), c)
                    fresh = jnp.concatenate([jnp.zeros_like(fixed), fixed], axis=1) - two[:BLOCK]
                    pbuf[h, p * unit + b * BLOCK:p * unit + (b + 1) * BLOCK, :] = (
                        two[BLOCK:] + mm(scores[at, at], fresh))
                    carry[h] = jnp.exp(last) * c + mm(fall, fresh, ((0,), (0,)))
        for h in some:
            cbuf[h] = carry[h]

    def pool():
        at_row = lax.broadcasted_iota(jnp.int32, (length, group_dim), 0) + sp * length
        for i in range(groups):
            at = slice(i * group_dim, (i + 1) * group_dim)
            x = raw[POOL, :, at]
            span = 2 * jnp.left_shift(1, lax.rem(tp * groups + i, 4))
            total = x
            window = jnp.zeros_like(x)
            for w in (2, 4, 8, 16):
                total = total + pltpu.roll(total, w // 2, 0)
                window = window + jnp.where(span == w, total, 0.0)
            tally = jnp.minimum(at_row + 1, span).astype(f32)
            pooled = (window[halo:] / tally - x[halo:]).astype(bf16)
            mixed = jnp.dot(pooled, mix_ref[i], preferred_element_type=f32)
            pool_out[:, at] = (mixed * scale_ref[:, at]).astype(bf16)

    cut = (heads + 1) // 2
    delta(range(cut))
    gather.forward(4)
    gather.finish(3)
    project(3)
    if cut < heads:
        delta(range(cut, heads))
    gather.forward(5)
    gather.finish(4)
    project(4)

    def state_copy(h):
        return pltpu.make_async_remote_copy(
            src_ref=s_out.at[h], dst_ref=s_in.at[h], send_sem=st_s.at[h], recv_sem=st_r.at[h],
            device_id={"sp": lax.rem(sp + 1, n_sp)}, device_id_type=MESH)

    @pl.when(sp == 0)
    def _():
        s_in[...] = jnp.zeros_like(s_in)

    gather.forward(6)
    gather.finish(5)
    pool()
    for h in range(heads):
        @pl.when(sp > 0)
        def _():
            state_copy(h).wait_recv()
        s_out[h] = (mm(cbuf[h, :, :head_dim], s_in[h].astype(f32)) + cbuf[h, :, head_dim:]).astype(bf16)

        @pl.when(sp < n_sp - 1)
        def _():
            state_copy(h).start()
    gather.flush(6)
    for h in range(heads):
        at = slice(h * head_dim, (h + 1) * head_dim)
        attended = mm(pbuf[h, :, :head_dim], s_in[h].astype(f32)) + pbuf[h, :, head_dim:]
        scale = lax.rsqrt(jnp.mean(attended * attended, axis=-1, keepdims=True) + eps)
        delta_out[:, at] = (attended * scale * dgain_ref[...] * silu(raw[GATE, halo:, at])).astype(bf16)
    gather.finish(6)

    def rs_copy(s, d, owner, dest):
        return pltpu.make_async_remote_copy(
            src_ref=part.at[s, pl.ds(pl.multiple_of(dest * rows, 16), rows)], dst_ref=rsbuf.at[s, owner],
            send_sem=rs_s.at[s, d - 1], recv_sem=rs_r.at[s, d - 1],
            device_id={"tp": lax.rem(tp + d, n_tp)}, device_id_type=MESH)

    for s in range(n_sp):
        part[s] = (jnp.dot(pool_out[...], wbuf[OUT_POOL, s], preferred_element_type=f32)
                   + jnp.dot(delta_out[...], wbuf[OUT_DELTA, s], preferred_element_type=f32)).astype(bf16)
        for d in range(1, n_tp):
            rs_copy(s, d, tp, lax.rem(tp + d, n_tp)).start()
    cols = wbuf.shape[3]
    for s in range(n_sp):
        total = part[s, pl.ds(pl.multiple_of(tp * rows, 16), rows)].astype(f32)
        for d in range(1, n_tp):
            owner = lax.rem(tp - d + n_tp, n_tp)
            rs_copy(s, d, owner, tp).wait_recv()
            total = total + rsbuf[s, owner].astype(f32)
        out_ref[:, s * cols:(s + 1) * cols] = total.astype(bf16)
    drain()
    for w in range(count):
        gather.drain(w)

    @pl.when(sp < n_sp - 1)
    def _():
        for h in range(heads):
            state_copy(h).wait_send()
    for s in range(n_sp):
        for d in range(1, n_tp):
            rs_copy(s, d, tp, lax.rem(tp + d, n_tp)).wait_send()


def per_device(
    tokens,
    norm_gain,
    w_pool_in,
    w_query,
    w_key,
    w_value,
    w_gate,
    w_beta,
    w_decay,
    conv_weight,
    a_log,
    decay_extra,
    w_mix,
    pool_scale,
    delta_gain,
    w_out_pool,
    w_out_delta,
):
    n_sp, n_fs, n_tp = (lax.axis_size(a) for a in ("sp", "fs", "tp"))
    weights = (w_key, w_query, w_value, w_pool_in, w_gate, w_out_pool, w_out_delta)
    rows, width = tokens.shape
    depth, cols = w_key.shape
    heads = a_log.shape[0]
    head_dim = cols // heads
    length = n_tp * rows
    count = len(weights)
    lanes = 128
    lane = lax.axis_index("tp")

    def own(w):
        return lax.dynamic_slice_in_dim(w, lane * heads, heads, 1)

    def wide(x):
        return jnp.pad(x, ((0, 0), (0, lanes - x.shape[1])))

    w_bd = wide(jnp.concatenate([own(w_decay), own(w_beta)], axis=1))
    slots = max(1, 2 ** len(share_bits(n_fs)) - 1)
    side = max(1, n_tp - 1)
    dma = pltpu.SemaphoreType.DMA
    vmem, anywhere = pl.BlockSpec(memory_space=pltpu.VMEM), pl.BlockSpec(memory_space=pl.ANY)
    return pl.pallas_call(
        functools.partial(mixer_kernel, n_sp, n_fs, n_tp),
        out_shape=jax.ShapeDtypeStruct((rows, width), bf16),
        in_specs=[anywhere] + [vmem] * 8 + [anywhere] * count,
        out_specs=vmem,
        scratch_shapes=[
            pltpu.VMEM((halo + length, width), bf16),
            pltpu.VMEM((halo + length, width), bf16),
            pltpu.VMEM((count, n_sp, depth, cols), bf16),
            pltpu.VMEM((5, halo + length, cols), f32),
            pltpu.VMEM((length, cols), bf16),
            pltpu.VMEM((length, cols), bf16),
            pltpu.VMEM((heads, length, 2 * head_dim), f32),
            pltpu.VMEM((heads, head_dim, 2 * head_dim), f32),
            pltpu.VMEM((heads, head_dim, head_dim), bf16),
            pltpu.VMEM((heads, head_dim, head_dim), bf16),
            pltpu.VMEM((n_sp, length, cols), bf16),
            pltpu.VMEM((n_sp, n_tp, rows, cols), bf16),
            dma((count + 1,)), dma((side,)), dma((side,)), dma((n_tp,)), dma((n_tp,)),
            dma((count, n_sp, 2)), dma((count, n_sp)), dma((count, n_sp, slots)), dma((count, n_sp, slots)),
            dma((heads,)), dma((heads,)), dma((n_sp, side)), dma((n_sp, side)),
        ],
        compiler_params=pltpu.CompilerParams(collective_id=0, has_side_effects=True, vmem_limit_bytes=56 << 20),
    )(tokens, norm_gain.reshape(1, -1), w_bd, conv_weight, wide(a_log.reshape(1, -1)), wide(decay_extra), w_mix,
      pool_scale.reshape(1, -1), delta_gain.reshape(1, -1), *weights)


def solution(mesh):
    placed = (
        P(("fs", "sp", "tp"), None),
        P(),
        P("sp", "tp"),
        P("sp", "tp"),
        P("sp", "tp"),
        P("sp", "tp"),
        P("sp", "tp"),
        P(),
        P(),
        P(None, None, "tp"),
        P("tp"),
        P(("fs", "sp"), "tp"),
        P("tp", None, None),
        P("tp"),
        P(),
        P("tp", "sp"),
        P("tp", "sp"),
    )
    return jax.shard_map(
        per_device,
        mesh=mesh,
        in_specs=placed,
        out_specs=P(("fs", "sp", "tp"), None),
        check_vma=False,
    )
```

time: 251 us -> 141 us (0.56); the launches traced: 246 us -> 141 us
  matrix products: 39.8 us -> 0 us
  waiting for transfers between devices: 37.2 us -> 0 us
  Pallas kernels: 106 us -> 133 us
  local copies, waits for them, and re-layouts: 26.3 us -> 7.79 us
  other arithmetic: 18.5 us -> 0.02 us
  between operations: 14.4 us -> 0.05 us
  starting transfers between devices: 3.88 us -> 0 us
    dot_general x52 -> x0, matrix products: 39.8 us -> none  [the longest x4 5.14 us: compose_step(): jnp.einsum('hcd,hce->hde', key_decayed, fresh, precision=highest)]
    pallas_call x1, Pallas kernels: 106 us -> 133 us  [per_device(): pl.pallas_call(functools.partial(mixer_kernel, n_sp, n_fs, n_tp), out_sha...]
    reduce_scatter x1 -> x0, waiting for transfers between devices: 22 us -> none  [per_device(): lax.psum_scatter(lax.optimization_barrier(value_partial_rows.astype(jnp.b...]
    ppermute x3 -> x0, waiting for transfers between devices: 15.2 us -> none  [from_behind(): return lax.ppermute(block, axis, route)]
    unnamed x87 -> x6, local copies, waits for them, and re-layouts: 9.68 us -> 2.67 us
    transpose x4 -> x0, local copies, waits for them, and re-layouts: 6.98 us -> none  [the longest x3 6.8 us: per_device(): jnp.transpose(gathered_out[i], (1, 0, 2)).reshape(w_out_pool.shape[0], -1)]
    exp x8 -> x0, local copies, waits for them, and re-layouts: 5.51 us -> none  [the longest x4 2.77 us: compose_step(): fade = jnp.exp(last_gate)[:, None, None]]
    ppermute x3 -> x0, starting transfers between devices: 3.88 us -> none  [from_behind(): return lax.ppermute(block, axis, route)]
  transfers between devices with their start and end apart: 4 -> 0, of which waited for: 4 -> 0; matrix products, arithmetic and copies ran while one was open for 0% -> 0% of each run, Pallas kernels for 0% -> 0%
where the time goes in v2:
time: 141 us
  Pallas kernels  133 us (94%)
  local copies, waits for them, and re-layouts  7.79 us (6%)
    pallas_call x1, Pallas kernels, per_device(): pl.pallas_call(functools.partial(mixer_kernel, n_sp, n_fs, n_tp), out_sha...  133 us

profile of v2, /device:TPU:31, one launch (start us, length us, event | category | flops | bytes accessed | tf_op | source)
XLA Modules:
  0.0 140.7 jit_solution(8102866013254028343)
XLA Ops:
  0.0 0.0 copy-start
  0.0 1.2 pad.13.refs_4_
  1.2 1.3 reshape.12.refs_1_
  2.5 0.0 copy-done
  2.5 0.8 constant_dynamic-slice_fusion
  3.3 0.0 copy-start.1
  3.3 0.6 copy-done.1
  4.0 0.1 copy.22
  4.1 0.7 pad.14.refs_5_
  4.8 0.3 copy.21
  5.1 0.9 pad.12.refs_2_
  6.0 132.8 %shard_map.163 = bf16[128,2048]{1,0:T(8,128)(2,1)} custom-call(bf16[128,2048]{1,0:T(8,128)(2,1)} %refs_0_.1, bf16[1,2048]{1,0:T(2,128)(2,1)} %reshape.12.refs_1_, bf16[2048,128]{1,0:T(8,128)(2,1)} %pad.12.refs_2_, f32[3,4,512]{2,1,0:T(4,128)} %refs_3_.1, f32[1,128]{1,0:T(1,128)} %pad.13.refs_4_, f32[256,128]{1,0:T(8,128)} %pad.14.refs_5_, ...), custom_call_target="tpu_custom_call" | custom-call | tf_op jit(solution)/shard_map/pallas_call | solution.py:505
  138.8 1.9 %copy.24 = bf16[128,2048]{1,0:T(8,128)(2,1)} copy(bf16[128,2048]{1,0:T(8,128)(2,1)} %shard_map.163) | data formatting | bytes 1048576
  (1 shorter events, 0.0 us)
Async XLA Ops:
  0.0 2.5 %copy-start = (bf16[2048,8]{0,1:T(8,128)(2,1)S(1)}, bf16[2048,8]{0,1:T(8,128)(2,1)}, u32[]{:S(2)}) copy-start(bf16[2048,8]{0,1:T(8,128)(2,1)} %param.24) | copy-start | bytes 98308
  3.3 0.7 copy-start.1

commit v3 on v2

--- a/solution.py
+++ b/solution.py
@@ -284,6 +284,7 @@
         raw[w] = total.astype(bf16).astype(f32)
 
     gather.forward(0)
+    gather.forward(1)
     finish()
     lax.fori_loop(0, tokbuf.shape[0] // 16, norm, 0)
     pre = jnp.dot(normbuf[...], wbd_ref[...], preferred_element_type=f32)[halo:]
@@ -296,7 +297,6 @@
     cum = mm(tri, log_gate)
     cum_t = cum.T
 
-    gather.forward(1)
     gather.finish(0)
     project(0)
     gather.forward(2)
@@ -365,11 +365,11 @@
                     last = g[(b + 1) * BLOCK - 1:(b + 1) * BLOCK]
                     fall = k[at] * jnp.exp(last - g[at])
                     c = carry[h]
-                    two = mm(jnp.concatenate([kw, qg[at]], axis=0), c)
+                    two = mm(jnp.concatenate([kw, qg[at]], axis=0), c, precision=None)
                     fresh = jnp.concatenate([jnp.zeros_like(fixed), fixed], axis=1) - two[:BLOCK]
                     pbuf[h, p * unit + b * BLOCK:p * unit + (b + 1) * BLOCK, :] = (
-                        two[BLOCK:] + mm(scores[at, at], fresh))
-                    carry[h] = jnp.exp(last) * c + mm(fall, fresh, ((0,), (0,)))
+                        two[BLOCK:] + mm(scores[at, at], fresh, precision=None))
+                    carry[h] = jnp.exp(last) * c + mm(fall, fresh, ((0,), (0,)), None)
         for h in some:
             cbuf[h] = carry[h]
 
@@ -416,7 +416,7 @@
         @pl.when(sp > 0)
         def _():
             state_copy(h).wait_recv()
-        s_out[h] = (mm(cbuf[h, :, :head_dim], s_in[h].astype(f32)) + cbuf[h, :, head_dim:]).astype(bf16)
+        s_out[h] = (mm(cbuf[h, :, :head_dim], s_in[h].astype(f32), precision=None) + cbuf[h, :, head_dim:]).astype(bf16)
 
         @pl.when(sp < n_sp - 1)
         def _():
@@ -424,7 +424,7 @@
     gather.flush(6)
     for h in range(heads):
         at = slice(h * head_dim, (h + 1) * head_dim)
-        attended = mm(pbuf[h, :, :head_dim], s_in[h].astype(f32)) + pbuf[h, :, head_dim:]
+        attended = mm(pbuf[h, :, :head_dim], s_in[h].astype(f32), precision=None) + pbuf[h, :, head_dim:]
         scale = lax.rsqrt(jnp.mean(attended * attended, axis=-1, keepdims=True) + eps)
         delta_out[:, at] = (attended * scale * dgain_ref[...] * silu(raw[GATE, halo:, at])).astype(bf16)
     gather.finish(6)

time: 141 us -> 136 us (0.965)
  Pallas kernels: 133 us -> 128 us
    pallas_call x1, Pallas kernels: 133 us -> 128 us  [per_device(): pl.pallas_call(functools.partial(mixer_kernel, n_sp, n_fs, n_tp), out_sha...]
where the time goes in v3:
time: 136 us
  Pallas kernels  128 us (94%)
  local copies, waits for them, and re-layouts  7.79 us (6%)
    pallas_call x1, Pallas kernels, per_device(): pl.pallas_call(functools.partial(mixer_kernel, n_sp, n_fs, n_tp), out_sha...  128 us
    pad x3, local copies, waits for them, and re-layouts, wide(): return jnp.pad(x, ((0, 0), (0, lanes - x.shape[1])))  2.78 us

profile of v3, /device:TPU:31, one launch (start us, length us, event | category | flops | bytes accessed | tf_op | source)
XLA Modules:
  0.0 135.7 jit_solution(8396402994204324408)
XLA Ops:
  0.0 0.0 copy-start
  0.0 1.2 pad.13.refs_4_
  1.2 1.3 reshape.12.refs_1_
  2.5 0.0 copy-done
  2.5 0.8 constant_dynamic-slice_fusion
  3.3 0.0 copy-start.1
  3.3 0.6 copy-done.1
  4.0 0.1 copy.22
  4.1 0.7 pad.14.refs_5_
  4.8 0.3 copy.21
  5.1 0.9 pad.12.refs_2_
  6.0 127.9 %shard_map.163 = bf16[128,2048]{1,0:T(8,128)(2,1)} custom-call(bf16[128,2048]{1,0:T(8,128)(2,1)} %refs_0_.1, bf16[1,2048]{1,0:T(2,128)(2,1)} %reshape.12.refs_1_, bf16[2048,128]{1,0:T(8,128)(2,1)} %pad.12.refs_2_, f32[3,4,512]{2,1,0:T(4,128)} %refs_3_.1, f32[1,128]{1,0:T(1,128)} %pad.13.refs_4_, f32[256,128]{1,0:T(8,128)} %pad.14.refs_5_, ...), custom_call_target="tpu_custom_call" | custom-call | tf_op jit(solution)/shard_map/pallas_call | solution.py:505
  133.8 1.9 %copy.24 = bf16[128,2048]{1,0:T(8,128)(2,1)} copy(bf16[128,2048]{1,0:T(8,128)(2,1)} %shard_map.163) | data formatting | bytes 1048576
  (1 shorter events, 0.0 us)
Async XLA Ops:
  0.0 2.5 %copy-start = (bf16[2048,8]{0,1:T(8,128)(2,1)S(1)}, bf16[2048,8]{0,1:T(8,128)(2,1)}, u32[]{:S(2)}) copy-start(bf16[2048,8]{0,1:T(8,128)(2,1)} %param.24) | copy-start | bytes 98308
  3.3 0.7 copy-start.1
